TPU v7x, 512 devices: a whole 4x4x16 slice. The times are simulated.
512 devices in a mesh: fs: 64 (over z, y), tp: 8 (over x, core).
Axes of the slice: x: 4, y: 4, z: 16, core: 2. Of those that a mesh axis runs over, the one named last changes fastest.
Arguments:
- tokens: bfloat16 [20480, 2048], P('fs'), may hold values from -6 to 6
- w_gate: bfloat16 [2048, 5632], P('fs', 'tp'), may hold values from -0.125 to 0.125
- w_up: bfloat16 [2048, 5632], P('fs', 'tp'), may hold values from -0.125 to 0.125
- w_down: bfloat16 [5632, 2048], P('tp', 'fs'), may hold values from -0.078125 to 0.078125
- w_mix_in: bfloat16 [2048, 1024], P('fs', 'tp'), may hold values from -0.125 to 0.125
- w_mix_out: bfloat16 [1024, 2048], P('tp', 'fs'), may hold values from -0.1875 to 0.1875
- pool_w: bfloat16 [8, 128, 128], P('tp'), may hold values from -0.5 to 0.5
- pool_scale: bfloat16 [1024], P('tp'), may hold values from 0.099609375 to 1.8984375
- norm_gains: float32 [6, 2048], replicated, may hold values from 0.1 to 1.9
Outputs:
- layer_out: bfloat16 [20480, 2048], P(('fs', 'tp'))
All inputs are finite; a program needn't handle non-finite values.
Results may differ from a plain program's by a relative error of at most 0.018.
Values may be sent and summed in bfloat16 or wider, within the bound.
No kernel may reach another device: no remote copies, remote signals or barrier semaphores. Data moves between devices by JAX's collectives and lax.ppermute only.
A program may use at most 64 MiB of HBM per device.

v0:
```python
import functools

import jax
import jax.numpy as jnp
from jax import lax
from jax.experimental import pallas as pl
from jax.experimental.pallas import tpu as pltpu
from jax.sharding import PartitionSpec as P


LEN = 64
NZ, NY = 16, 4
BF = jnp.bfloat16
F32 = jnp.float32
VMEM = pl.BlockSpec(memory_space=pltpu.VMEM)
SMEM = pl.BlockSpec(memory_space=pltpu.SMEM)


def limit(mib):
    return pltpu.CompilerParams(vmem_limit_bytes=mib * 1024 * 1024)


OFFSETS = tuple(range(-8, 8))
BATCHES = ((0, -1, 1, -2, 2, -3, 3, -4, 4, -5, 5), (-6, 6, -7, 7, -8))
HBM = pl.BlockSpec(memory_space=pltpu.HBM)


def fs_shift(dy, dz):
    return [
        (z * NY + y, ((z + dz) % NZ) * NY + (y + dy) % NY) for z in range(NZ) for y in range(NY)
    ]


def shift(array, dy=0, dz=0):
    return lax.ppermute(array, "fs", fs_shift(dy, dz))


def rolled(array, first_block):
    twice = jnp.concatenate([array, array], axis=1)
    return lax.dynamic_slice_in_dim(twice, first_block * 128, array.shape[1], 1)


def pack_kernel(gate_in, up_in, mix_in, mix_out, down_in, first_ref, second_ref, *scratch):
    held, sems = scratch[:5], scratch[5]
    copies = []
    for k, (src, dst) in enumerate(zip((gate_in, up_in, mix_in, mix_out, down_in), held)):
        copies.append(pltpu.make_async_copy(src, dst, sems.at[k]))
        copies[-1].start()
    for copy in copies:
        copy.wait()
    gate_ref, up_ref, in_ref, out_ref, down_ref = held
    width = gate_ref.shape[1]
    whole = width // 128 * 128
    first_ref[:, :whole] = gate_ref[:, :whole]
    first_ref[:, whole : 2 * whole] = up_ref[:, :whole]
    first_ref[:, 2 * whole :] = jnp.concatenate([gate_ref[:, whole:], up_ref[:, whole:]], axis=1)
    second_ref[:, 0:128] = in_ref[...]
    second_ref[:, 128:256] = out_ref[...]
    second_ref[:, 256 : 256 + width] = down_ref[...]
    second_ref[:, 256 + width :] = jnp.zeros((32, width - 256), BF)


def pack(*weights):
    shape = jax.ShapeDtypeStruct((32, 2 * weights[0].shape[1]), BF)
    return pl.pallas_call(
        pack_kernel,
        out_shape=(shape, shape),
        in_specs=[HBM] * 5,
        out_specs=(VMEM, VMEM),
        scratch_shapes=[pltpu.VMEM(w.shape, BF) for w in weights] + [pltpu.SemaphoreType.DMA((5,))],
        compiler_params=limit(63),
        cost_estimate=pl.CostEstimate(flops=10**8, bytes_accessed=1 << 18, transcendentals=0),
        name="pack",
    )(*weights)


def by_core(core, blocks):
    even, odd = blocks[0::2], blocks[1::2]
    mine = [jnp.where(core == 0, a, b) for a, b in zip(even, odd)]
    other = [jnp.where(core == 0, b, a) for a, b in zip(even, odd)]
    return jnp.concatenate(mine + other, axis=0)


def first_norm_kernel(at_ref, x_ref, gain_ref, out_ref):
    rows, depth = x_ref.shape
    tile = rows // 8
    block, core = at_ref[0], at_ref[1]
    halves = ([], [])
    for i in range(4):
        x0 = x_ref[2 * i * tile : (2 * i + 1) * tile, :].astype(F32)
        x1 = x_ref[(2 * i + 1) * tile : (2 * i + 2) * tile, :].astype(F32)
        for k, x in enumerate((x0, x1)):
            scale = lax.rsqrt(jnp.mean(x * x, axis=-1, keepdims=True) + 1e-06)
            halves[k].append(scale)
    for p in range(depth // 128):
        start = pl.multiple_of(lax.rem(block + p, depth // 128) * 128, 128)
        gain = gain_ref[0:1, p * 128 : (p + 1) * 128]
        mine, other = [], []
        for i in range(4):
            x0 = x_ref[2 * i * tile : (2 * i + 1) * tile, pl.ds(start, 128)].astype(F32)
            x1 = x_ref[(2 * i + 1) * tile : (2 * i + 2) * tile, pl.ds(start, 128)].astype(F32)
            x0 = (x0 * halves[0][i] * gain).astype(BF)
            x1 = (x1 * halves[1][i] * gain).astype(BF)
            mine.append(jnp.where(core == 0, x0, x1))
            other.append(jnp.where(core == 0, x1, x0))
        for i in range(4):
            out_ref[i * tile : (i + 1) * tile, p * 128 : (p + 1) * 128] = mine[i]
            out_ref[(4 + i) * tile : (5 + i) * tile, p * 128 : (p + 1) * 128] = other[i]


def first_norm(at, tokens, gain):
    return pl.pallas_call(
        first_norm_kernel,
        out_shape=jax.ShapeDtypeStruct(tokens.shape, BF),
        in_specs=[SMEM, VMEM, VMEM],
        out_specs=VMEM,
        compiler_params=limit(8),
        cost_estimate=pl.CostEstimate(flops=10**9, bytes_accessed=3 << 20, transcendentals=0),
        name="first_norm",
    )(at, tokens, gain)


def rms_scale(values, gain):
    return values * lax.rsqrt(jnp.mean(values * values, axis=-1, keepdims=True) + 1e-06) * gain


def settle_kernel(factor, row, parts_ref, stream_ref, gain_ref, new_ref, normed_ref):
    total = parts_ref[0].astype(F32)
    for k in range(1, parts_ref.shape[0]):
        total = total + parts_ref[k].astype(F32)
    stream = stream_ref[...] + factor * rms_scale(total, gain_ref[row : row + 1, :])
    new_ref[...] = stream
    normed = rms_scale(stream, gain_ref[row + 1 : row + 2, :]).astype(BF)
    for k in range(normed_ref.shape[0]):
        normed_ref[k] = normed


def settle(parts, stream, gains, row, factor):
    return pl.pallas_call(
        functools.partial(settle_kernel, factor, row),
        out_shape=(
            jax.ShapeDtypeStruct(stream.shape, F32),
            jax.ShapeDtypeStruct((4, *stream.shape), BF),
        ),
        in_specs=[VMEM] * 3,
        out_specs=(VMEM, VMEM),
        compiler_params=limit(6),
        cost_estimate=pl.CostEstimate(flops=10**8, bytes_accessed=1 << 20, transcendentals=0),
        name="settle",
    )(parts, stream, gains)


def finish_kernel(at_ref, parts_ref, stream_ref, gain_ref, out_ref):
    total = parts_ref[0].astype(F32)
    for k in range(1, parts_ref.shape[0]):
        total = total + parts_ref[k].astype(F32)
    result = (stream_ref[...] + 0.5 * rms_scale(total, gain_ref[5:6, :])).astype(BF)
    blocks = result.shape[1] // 128
    for p in range(blocks):
        start = pl.multiple_of(lax.rem(at_ref[0] + p, blocks) * 128, 128)
        out_ref[:, pl.ds(start, 128)] = result[:, p * 128 : (p + 1) * 128]


def finish(at, parts, stream, gains):
    return pl.pallas_call(
        finish_kernel,
        out_shape=jax.ShapeDtypeStruct(stream.shape, BF),
        in_specs=[SMEM] + [VMEM] * 3,
        out_specs=VMEM,
        compiler_params=limit(6),
        cost_estimate=pl.CostEstimate(flops=10**8, bytes_accessed=1 << 20, transcendentals=0),
        name="finish",
    )(at, parts, stream, gains)


def act(gate, up):
    return (gate / (1.0 + jnp.exp(-gate)) * up).astype(BF)


def gated_product(x, w_ref, out_ref):
    width = out_ref.shape[1]
    whole = width // 128 * 128
    at = 0
    while at < whole:
        n = min(256, whole - at)
        gate = jnp.dot(x, w_ref[:, at : at + n], preferred_element_type=F32)
        up = jnp.dot(x, w_ref[:, whole + at : whole + at + n], preferred_element_type=F32)
        out_ref[:, at : at + n] = act(gate, up)
        at += n
    both = jnp.dot(x, w_ref[:, 2 * whole :], preferred_element_type=F32)
    out_ref[:, whole:] = act(both[:, : width - whole], both[:, width - whole :])


def gated_first_kernel(x_ref, *refs):
    payloads, out_ref, w_ref = refs[:NZ], refs[-2], refs[-1]
    for k in range(NZ):
        w_ref[k * 128 : (k + 1) * 128, :] = payloads[k][0:128, :]
    gated_product(x_ref[...], w_ref, out_ref)


def gated_then_kernel(x_ref, w_ref, out_ref):
    gated_product(x_ref[...], w_ref, out_ref)


def gated(x, weights, width):
    rows, depth = x.shape
    hidden = jax.ShapeDtypeStruct((rows, width), BF)
    whole = jax.ShapeDtypeStruct((depth, 2 * width), BF)
    first = len(weights) > 1
    return pl.pallas_call(
        gated_first_kernel if first else gated_then_kernel,
        out_shape=(hidden, whole) if first else hidden,
        in_specs=[VMEM] * (1 + len(weights)),
        out_specs=(VMEM, VMEM) if first else VMEM,
        compiler_params=limit(16 if first else 10),
        cost_estimate=pl.CostEstimate(
            flops=4 * rows * depth * width, bytes_accessed=8 << 20, transcendentals=0
        ),
        name="gated",
    )(x, *weights)


def absorb_kernel(places, x_ref, *refs):
    n = len(places)
    blocks, total_ref = refs[:n], refs[-1]
    x = [x_ref[:, place * 128 : (place + 1) * 128] for place in places]
    x = x[0] if n == 1 else jnp.concatenate(x, axis=1)
    width = total_ref.shape[1]
    for at in range(0, width, 256):
        end = min(width, at + 256)
        w = [block[0:128, at:end] for block in blocks]
        w = w[0] if n == 1 else jnp.concatenate(w, axis=0)
        part = jnp.dot(x, w, preferred_element_type=F32)
        total_ref[:, at:end] = part if len(refs) == n + 1 else refs[n][:, at:end] + part


def absorb(x, blocks, places, total=None):
    rows, width, n = x.shape[0], blocks[0].shape[1], len(blocks)
    carried = () if total is None else (total,)
    return pl.pallas_call(
        functools.partial(absorb_kernel, places),
        out_shape=jax.ShapeDtypeStruct((rows, width), F32),
        in_specs=[VMEM] * (1 + n + len(carried)),
        out_specs=VMEM,
        input_output_aliases={} if total is None else {1 + n: 0},
        compiler_params=limit(6),
        cost_estimate=pl.CostEstimate(
            flops=2 * rows * width * 128 * n, bytes_accessed=n << 19, transcendentals=0
        ),
        name="absorb",
    )(x, *blocks, *carried)


def silu_kernel(total_ref, mine_ref, other_ref):
    half, width = mine_ref.shape
    whole = width // 128 * 128
    for k, ref in enumerate((mine_ref, other_ref)):
        rows = slice(k * half, (k + 1) * half)
        ref[:, :whole] = act(total_ref[rows, :whole], total_ref[rows, whole : 2 * whole])
        both = total_ref[rows, 2 * whole :]
        ref[:, whole:] = act(both[:, : width - whole], both[:, width - whole :])


def silu(total):
    rows, width = total.shape
    return pl.pallas_call(
        silu_kernel,
        out_shape=(jax.ShapeDtypeStruct((rows // 2, width // 2), BF),) * 2,
        in_specs=[VMEM],
        out_specs=(VMEM, VMEM),
        compiler_params=limit(4),
        cost_estimate=pl.CostEstimate(flops=10**8, bytes_accessed=1 << 20, transcendentals=0),
        name="silu",
    )(total)


def assemble_kernel(y_ref, *refs):
    ins, mix_ref, down_ref = refs[:-2], refs[-2], refs[-1]
    y = y_ref[0]
    width = mix_ref.shape[1] + down_ref.shape[1]
    for k, batch in enumerate(BATCHES):
        for j in range(NY):
            owner = lax.rem(y - j + NY, NY)
            src = ins[NY * k + j]
            for i, offset in enumerate(batch):
                start = pl.multiple_of(OFFSETS.index(offset) * 128 + owner * 32, 32)
                mix_ref[pl.ds(start, 32), :] = src[i * 32 : (i + 1) * 32, 0:256]
                down_ref[pl.ds(start, 32), :] = src[i * 32 : (i + 1) * 32, 256:width]


def assemble(y, pieces, down_width):
    rows = NZ * NY * 32
    return pl.pallas_call(
        assemble_kernel,
        out_shape=(
            jax.ShapeDtypeStruct((rows, 256), BF),
            jax.ShapeDtypeStruct((rows, down_width), BF),
        ),
        in_specs=[SMEM] + [VMEM] * len(pieces),
        out_specs=(VMEM, VMEM),
        compiler_params=limit(14),
        cost_estimate=pl.CostEstimate(flops=10**8, bytes_accessed=8 << 20, transcendentals=0),
        name="assemble",
    )(y, *pieces)


def down_kernel(h_ref, w_ref, out_ref):
    h = h_ref[...]
    for at in range(0, w_ref.shape[0], 256):
        out_ref[:, at : at + 256] = lax.dot_general(
            h, w_ref[at : at + 256, :], (((1,), (1,)), ((), ())), preferred_element_type=F32
        ).astype(BF)


def down(hidden, w):
    rows, out = hidden.shape[0], w.shape[0]
    return pl.pallas_call(
        down_kernel,
        out_shape=jax.ShapeDtypeStruct((rows, out), BF),
        in_specs=[VMEM, VMEM],
        out_specs=VMEM,
        compiler_params=limit(14),
        cost_estimate=pl.CostEstimate(
            flops=2 * rows * out * w.shape[1], bytes_accessed=4 << 20, transcendentals=0
        ),
        name="down",
    )(hidden, w)


def pair_kernel(a_ref, b_ref, out_ref):
    rows = out_ref.shape[1]
    for k in range(out_ref.shape[0]):
        at = slice(k * rows, (k + 1) * rows)
        out_ref[k] = (a_ref[at, :].astype(F32) + b_ref[at, :].astype(F32)).astype(BF)


def pair_sum(a, b):
    return pl.pallas_call(
        pair_kernel,
        out_shape=jax.ShapeDtypeStruct((4, a.shape[0] // 4, a.shape[1]), BF),
        in_specs=[VMEM] * 2,
        out_specs=VMEM,
        compiler_params=limit(4),
        cost_estimate=pl.CostEstimate(flops=10**8, bytes_accessed=1 << 20, transcendentals=0),
        name="pair_sum",
    )(a, b)


def mixer_kernel(kind_ref, mine_ref, other_ref, w_ref, pool_ref, scale_ref, keep_ref, send_ref):
    rows = 2 * mine_ref.shape[0]
    tile = rows // 8
    kind, core = kind_ref[0], kind_ref[1]
    x = jnp.concatenate([mine_ref[...], other_ref[...]], axis=0)
    values = jnp.dot(x, w_ref[:, 0:128], preferred_element_type=F32)
    values = values.astype(BF).astype(F32)
    in_order = []
    for i in range(4):
        mine = values[i * tile : (i + 1) * tile]
        other = values[(4 + i) * tile : (5 + i) * tile]
        in_order += [jnp.where(core == 0, mine, other), jnp.where(core == 0, other, mine)]
    values = jnp.concatenate(in_order, axis=0)
    place = lax.broadcasted_iota(jnp.int32, (rows, 128), 0) % LEN
    total = values
    chosen = jnp.zeros_like(values)
    for slot in range(4):
        lag = 2**slot
        earlier = jnp.concatenate([jnp.zeros((lag, 128), F32), total[: rows - lag]], axis=0)
        total = total + jnp.where(place >= lag, earlier, 0.0)
        window = 2 * lag
        mean = total / jnp.minimum(place + 1, window).astype(F32)
        chosen = jnp.where(kind == slot, mean, chosen)
    deviation = (chosen - values).astype(BF)
    mixed = jnp.dot(deviation, pool_ref[...], preferred_element_type=F32)
    mixed = mixed * scale_ref[...].astype(F32)
    mixed = by_core(core, [mixed[i * tile : (i + 1) * tile] for i in range(8)]).astype(BF)
    for at in range(0, w_ref.shape[0], 256):
        share = lax.dot_general(
            mixed, w_ref[at : at + 256, 128:256], (((1,), (1,)), ((), ())), preferred_element_type=F32
        ).astype(BF)
        keep_ref[:, at : at + 256] = share[: rows // 2]
        send_ref[:, at : at + 256] = share[rows // 2 :]


def mixer(kind, mine, other, w, pool_w, pool_scale):
    rows, depth = 2 * mine.shape[0], mine.shape[1]
    return pl.pallas_call(
        mixer_kernel,
        out_shape=(jax.ShapeDtypeStruct((rows // 2, depth), BF),) * 2,
        in_specs=[SMEM] + [VMEM] * 5,
        out_specs=(VMEM, VMEM),
        compiler_params=limit(14),
        cost_estimate=pl.CostEstimate(
            flops=4 * rows * depth * 128, bytes_accessed=4 << 20, transcendentals=0
        ),
        name="mixer",
    )(kind, mine, other, w, pool_w, pool_scale)


X_GROUPS = [[2 * x + core for x in range(4)] for core in range(2)]


def core_swap(array):
    return lax.ppermute(array, "tp", [(k, k ^ 1) for k in range(8)])


def shares_of_rows(mine, other):
    tiles = pair_sum(mine, core_swap(other))
    return lax.all_to_all(tiles, "tp", 0, 0, tiled=True, axis_index_groups=X_GROUPS)


def rows_of_all(copies):
    mine = lax.all_to_all(copies, "tp", 0, 0, tiled=True, axis_index_groups=X_GROUPS)
    mine = mine.reshape(-1, copies.shape[-1])
    return mine, core_swap(mine)


def body(tokens, w_gate, w_up, w_down, w_mix_in, w_mix_out, pool_w, pool_scale, norm_gains):
    tp_size, tp_at = lax.axis_size("tp"), lax.axis_index("tp")
    fs_at = lax.axis_index("fs")
    z, y = fs_at // NY, fs_at % NY
    own_rows = tokens.shape[0] // tp_size
    width = w_gate.shape[1]

    groups = [[k * NY + j for j in range(NY)] for k in range(NZ)]
    second_width = 256 + width
    first, second = pack(w_gate, w_up, w_mix_in, w_mix_out.T, w_down.T)
    first = lax.all_gather(first, "fs", axis=0, tiled=True, axis_index_groups=groups)

    first_block = lax.rem(z + 8, NZ)
    core = lax.rem(tp_at, 2)
    gains = rolled(norm_gains, first_block)
    numbers = jnp.stack([first_block, core, lax.rem(tp_at, 4), y]).astype(jnp.int32)

    first, late_tokens = lax.optimization_barrier((first, tokens))
    back = ahead = jnp.concatenate([first, second], axis=0)
    x = first_norm(numbers[0:2], late_tokens, gains)
    got = {0: back}
    total = None
    for k in range(1, 9):
        if k == 7:
            last_second = shift(back[128:, :second_width], dz=2)
        back = got[-k] = shift(back, dz=1)
        if k < 8:
            ahead = got[k] = shift(ahead, dz=-1)
        places = ([0] if k == 1 else []) + [-k] + ([k] if k < 8 else [])
        total = absorb(x, [got[p] for p in places], tuple(8 + p for p in places), total)
    payloads = [got[k] for k in OFFSETS]

    pieces = []
    for batch in BATCHES:
        own = [last_second if s == -8 else got[s][128:, :second_width] for s in batch]
        own = jnp.concatenate(own, axis=0)
        pieces += [own, shift(own, dy=1), shift(own, dy=2), shift(own, dy=-1)]
    mix_w, down_w = assemble(numbers[3:4], pieces, width)

    stream = lax.dynamic_slice_in_dim(late_tokens, tp_at * own_rows, own_rows, 0)
    stream = rolled(stream, first_block).astype(F32)
    hidden, other = silu(total)
    other, mine = down(other, down_w), down(hidden, down_w)
    parts = shares_of_rows(mine, other)
    stream, copies = settle(parts, stream, gains, 1, 0.5)
    kind = jnp.stack([numbers[2], numbers[1]])
    share = mixer(kind, *rows_of_all(copies), mix_w, pool_w[0], pool_scale[None])
    stream, copies = settle(shares_of_rows(*share), stream, gains, 3, 1.0)
    mine, other = rows_of_all(copies)
    hidden, gate_up = gated(mine, payloads, width)
    other = gated(other, [gate_up], width)
    other, mine = down(other, down_w), down(hidden, down_w)
    parts = shares_of_rows(mine, other)
    return finish(numbers[0:1], parts, stream, gains)


def solution(mesh):
    in_specs = (
        P("fs", None),
        P("fs", "tp"),
        P("fs", "tp"),
        P("tp", "fs"),
        P("fs", "tp"),
        P("tp", "fs"),
        P("tp", None, None),
        P("tp"),
        P(),
    )
    out_specs = P(("fs", "tp"), None)

    return jax.shard_map(body, mesh=mesh, in_specs=in_specs, out_specs=out_specs, check_vma=False)
```

profile of v0, /device:TPU:1, one launch (start us, length us, event | category | flops | bytes accessed | tf_op | source)
XLA Modules:
  0.0 267.4 jit_solution(2525936371063846140)
XLA Ops:
  1.7 11.1 %all_gather.3 = bf16[128,1408]{1,0:T(8,128)(2,1)S(1)} all-gather(bf16[32,1408]{1,0:T(8,128)(2,1)} %get-tuple-element.21), channel_id=1, replica_groups={{0,8,16,24},{32,40,48,56},{64,72,80,88},{96,104,112,120},{128,136,144,1..., dimensions={0}, use_global_device_ids=true | all-gather | bytes 450560 | tf_op jit(solution)/shard_map/all_gather | solution.py:427
  13.7 12.1 %collective-permute-start.8 = (bf16[160,1408]{1,0:T(8,128)(2,1)S(1)}, bf16[160,1408]{1,0:T(8,128)(2,1)S(1)}, u32[]{:S(2)}, u32[]{:S(2)}) collective-permute-start(bf16[160,1408]{1,0:T(8,128)(2,1)S(1)} %constant_dynamic-update-slice_fusion.refs_0_.refs_8_), channel_id=1, source_target_pairs={{0,480},{8,488},{16,496},{24,504},{32,0},{40,8},{48,16},{56,24},{6... | collective-permute-start | bytes 1351688 | tf_op jit(solution)/shard_map/ppermute | solution.py:35
  29.4 3.6 %collective-permute-done.8.refs_2_.refs_9_ = bf16[160,1408]{1,0:T(8,128)(2,1)S(1)} collective-permute-done((bf16[160,1408]{1,0:T(8,128)(2,1)S(1)}, bf16[160,1408]{1,0:T(8,128)(2,1)S(1)}, u32[]{:S(2)}, u32[]{:S(2)}) %collective-permute-start.8) | collective-permute-done | bytes 450592 | tf_op jit(solution)/shard_map/ppermute | solution.py:35
  33.0 5.3 %collective-permute-start.9 = (bf16[160,1408]{1,0:T(8,128)(2,1)S(1)}, bf16[160,1408]{1,0:T(8,128)(2,1)S(1)}, u32[]{:S(2)}, u32[]{:S(2)}) collective-permute-start(bf16[160,1408]{1,0:T(8,128)(2,1)S(1)} %collective-permute-done.8.refs_2_.refs_9_), channel_id=1, source_target_pairs={{0,480},{8,488},{16,496},{24,504},{32,0},{40,8},{48,16},{56,24},{6... | collective-permute-start | bytes 1351688 | tf_op jit(solution)/shard_map/ppermute | solution.py:35
  41.5 3.0 %collective-permute-done.9.refs_1_.refs_10_ = bf16[160,1408]{1,0:T(8,128)(2,1)S(1)} collective-permute-done((bf16[160,1408]{1,0:T(8,128)(2,1)S(1)}, bf16[160,1408]{1,0:T(8,128)(2,1)S(1)}, u32[]{:S(2)}, u32[]{:S(2)}) %collective-permute-start.9) | collective-permute-done | bytes 450592 | tf_op jit(solution)/shard_map/ppermute | solution.py:35
  44.5 5.3 %collective-permute-start.10 = (bf16[160,1408]{1,0:T(8,128)(2,1)S(1)}, bf16[160,1408]{1,0:T(8,128)(2,1)S(1)}, u32[]{:S(2)}, u32[]{:S(2)}) collective-permute-start(bf16[160,1408]{1,0:T(8,128)(2,1)S(1)} %collective-permute-done.9.refs_1_.refs_10_), channel_id=1, source_target_pairs={{0,480},{8,488},{16,496},{24,504},{32,0},{40,8},{48,16},{56,24},{6... | collective-permute-start | bytes 1351688 | tf_op jit(solution)/shard_map/ppermute | solution.py:35
  55.2 5.4 %collective-permute-start.11 = (bf16[160,1408]{1,0:T(8,128)(2,1)S(1)}, bf16[160,1408]{1,0:T(8,128)(2,1)S(1)}, u32[]{:S(2)}, u32[]{:S(2)}) collective-permute-start(bf16[160,1408]{1,0:T(8,128)(2,1)S(1)} %collective-permute-done.10.refs_1_.refs_11_), channel_id=1, source_target_pairs={{0,480},{8,488},{16,496},{24,504},{32,0},{40,8},{48,16},{56,24},{6... | collective-permute-start | bytes 1351688 | tf_op jit(solution)/shard_map/ppermute | solution.py:35
  65.9 5.0 %collective-permute-start.12 = (bf16[160,1408]{1,0:T(8,128)(2,1)S(1)}, bf16[160,1408]{1,0:T(8,128)(2,1)S(1)}, u32[]{:S(2)}, u32[]{:S(2)}) collective-permute-start(bf16[160,1408]{1,0:T(8,128)(2,1)S(1)} %collective-permute-done.11.refs_1_.refs_12_), channel_id=1, source_target_pairs={{0,480},{8,488},{16,496},{24,504},{32,0},{40,8},{48,16},{56,24},{6... | collective-permute-start | bytes 1351688 | tf_op jit(solution)/shard_map/ppermute | solution.py:35
  76.3 5.0 %collective-permute-start.13 = (bf16[160,1408]{1,0:T(8,128)(2,1)S(1)}, bf16[160,1408]{1,0:T(8,128)(2,1)S(1)}, u32[]{:S(2)}, u32[]{:S(2)}) collective-permute-start(bf16[160,1408]{1,0:T(8,128)(2,1)S(1)} %collective-permute-done.12.refs_1_.refs_13_), channel_id=1, source_target_pairs={{0,480},{8,488},{16,496},{24,504},{32,0},{40,8},{48,16},{56,24},{6... | collective-permute-start | bytes 1351688 | tf_op jit(solution)/shard_map/ppermute | solution.py:35
  86.4 3.3 %collective-permute-start.17 = (bf16[352,960]{1,0:T(8,128)(2,1)}, bf16[352,960]{1,0:T(8,128)(2,1)S(1)}, u32[]{:S(2)}, u32[]{:S(2)}) collective-permute-start(bf16[352,960]{1,0:T(8,128)(2,1)} %slice_dynamic-update-slice_fusion.3.refs_0_), channel_id=1, source_target_pairs={{0,24},{8,0},{16,8},{24,16},{32,56},{40,32},{48,40},{56,48},{64,88... | collective-permute-start | bytes 2027528 | tf_op jit(solution)/shard_map/ppermute | solution.py:35
  94.2 4.6 %collective-permute-start.14 = (bf16[160,1408]{1,0:T(8,128)(2,1)S(1)}, bf16[160,1408]{1,0:T(8,128)(2,1)S(1)}, u32[]{:S(2)}, u32[]{:S(2)}) collective-permute-start(bf16[160,1408]{1,0:T(8,128)(2,1)S(1)} %collective-permute-done.13.refs_1_.refs_14_), channel_id=1, source_target_pairs={{0,480},{8,488},{16,496},{24,504},{32,0},{40,8},{48,16},{56,24},{6... | collective-permute-start | bytes 1351688 | tf_op jit(solution)/shard_map/ppermute | solution.py:35
  103.6 5.7 %collective-permute-done.6.refs_0_.refs_1_ = bf16[160,1408]{1,0:T(8,128)(2,1)} collective-permute-done((bf16[160,1408]{1,0:T(8,128)(2,1)S(1)}, bf16[160,1408]{1,0:T(8,128)(2,1)}, u32[]{:S(2)}, u32[]{:S(2)}) %collective-permute-start.6) | collective-permute-done | bytes 450592 | tf_op jit(solution)/shard_map/ppermute | solution.py:35
  117.3 4.7 %collective-permute-start.21 = (bf16[160,960]{1,0:T(8,128)(2,1)}, bf16[160,960]{1,0:T(8,128)(2,1)}, u32[]{:S(2)}, u32[]{:S(2)}) collective-permute-start(bf16[160,960]{1,0:T(8,128)(2,1)} %constant_dynamic-update-slice_fusion.2.refs_4_), channel_id=1, source_target_pairs={{0,24},{8,0},{16,8},{24,16},{32,56},{40,32},{48,40},{56,48},{64,88... | collective-permute-start | bytes 921608 | tf_op jit(solution)/shard_map/ppermute | solution.py:35
  143.8 23.2 %collective-permute-start.22 = (bf16[160,2048]{1,0:T(8,128)(2,1)S(1)}, bf16[160,2048]{1,0:T(8,128)(2,1)S(1)}, u32[]{:S(2)}, u32[]{:S(2)}) collective-permute-start(bf16[160,2048]{1,0:T(8,128)(2,1)S(1)} %down.5), channel_id=1, source_target_pairs={{0,1},{1,0},{2,3},{3,2},{4,5},{5,4},{6,7},{7,6},{8,9},{9,8},{10,11... | collective-permute-start | bytes 1966088 | tf_op jit(solution)/shard_map/ppermute | solution.py:403
  169.8 4.2 %all-to-all-start = ((bf16[4,40,2048]{2,1,0:T(8,128)(2,1)}), bf16[4,40,2048]{2,1,0:T(8,128)(2,1)}, u32[]{:S(2)}, u32[]{:S(2)}) async-start(bf16[4,40,2048]{2,1,0:T(8,128)(2,1)} %copy-done.2), calls=%async_computation | async-start | bytes 1310720 | tf_op jit(solution)/shard_map/all_to_all | solution.py:408
  175.0 9.4 %all-to-all-done.parts_ref = bf16[4,40,2048]{2,1,0:T(8,128)(2,1)} async-done(((bf16[4,40,2048]{2,1,0:T(8,128)(2,1)}), bf16[4,40,2048]{2,1,0:T(8,128)(2,1)}, u32[]{:S(2)}, u32[]{:S(2)}) %all-to-all-start) | async-done | bytes 655392 | tf_op jit(solution)/shard_map/all_to_all | solution.py:408
  185.9 12.4 %all_to_all.25 = bf16[4,40,2048]{2,1,0:T(8,128)(2,1)} all-to-all(bf16[4,40,2048]{2,1,0:T(8,128)(2,1)S(1)} %get-tuple-element.28), channel_id=1, replica_groups={{0,2,4,6},{1,3,5,7},{8,10,12,14},{9,11,13,15},{16,18,20,22},{17,19,21,2..., dimensions={0} | all-to-all | bytes 1310720 | tf_op jit(solution)/shard_map/all_to_all | solution.py:412
  198.3 4.4 %collective-permute-start.23 = (bf16[160,2048]{1,0:T(8,128)(2,1)}, bf16[160,2048]{1,0:T(8,128)(2,1)}, u32[]{:S(2)}, u32[]{:S(2)}) collective-permute-start(bf16[160,2048]{1,0:T(8,128)(2,1)} %bitcast.6.mine_ref), channel_id=1, source_target_pairs={{0,1},{1,0},{2,3},{3,2},{4,5},{5,4},{6,7},{7,6},{8,9},{9,8},{10,11... | collective-permute-start | bytes 1966088 | tf_op jit(solution)/shard_map/ppermute | solution.py:403
  206.8 3.2 %mixer.1 = (bf16[160,2048]{1,0:T(8,128)(2,1)S(1)}, bf16[160,2048]{1,0:T(8,128)(2,1)S(1)}) custom-call(s32[2]{0:T(128)S(1)} %pad_add_fusion.kind_ref, bf16[160,2048]{1,0:T(8,128)(2,1)} %bitcast.6.mine_ref, bf16[160,2048]{1,0:T(8,128)(2,1)} %collective-permute-done.23.other_ref, bf16[2048,256]{1,0:T(8,128)(2,1)S(1)} %copy-done.37, ...), custom_call_target="tpu_custom_call" | custom-call | flops 335544320 | bytes 4194304 | tf_op jit(solution)/shard_map/mixer/pallas_call | solution.py:386
  214.2 13.3 %all_to_all.26.parts_ref = bf16[4,40,2048]{2,1,0:T(8,128)(2,1)S(1)} all-to-all(bf16[4,40,2048]{2,1,0:T(8,128)(2,1)S(1)} %pair_sum.4), channel_id=1, replica_groups={{0,2,4,6},{1,3,5,7},{8,10,12,14},{9,11,13,15},{16,18,20,22},{17,19,21,2..., dimensions={0} | all-to-all | bytes 1310720 | tf_op jit(solution)/shard_map/all_to_all | solution.py:408
  227.8 12.2 %all_to_all.27 = bf16[4,40,2048]{2,1,0:T(8,128)(2,1)S(1)} all-to-all(bf16[4,40,2048]{2,1,0:T(8,128)(2,1)S(1)} %get-tuple-element.33), channel_id=1, replica_groups={{0,2,4,6},{1,3,5,7},{8,10,12,14},{9,11,13,15},{16,18,20,22},{17,19,21,2..., dimensions={0} | all-to-all | bytes 1310720 | tf_op jit(solution)/shard_map/all_to_all | solution.py:412
  239.9 4.0 %collective-permute-start.25 = (bf16[160,2048]{1,0:T(8,128)(2,1)S(1)}, bf16[160,2048]{1,0:T(8,128)(2,1)S(1)}, u32[]{:S(2)}, u32[]{:S(2)}) collective-permute-start(bf16[160,2048]{1,0:T(8,128)(2,1)S(1)} %bitcast.10), channel_id=1, source_target_pairs={{0,1},{1,0},{2,3},{3,2},{4,5},{5,4},{6,7},{7,6},{8,9},{9,8},{10,11... | collective-permute-start | bytes 1966088 | tf_op jit(solution)/shard_map/ppermute | solution.py:403
  244.1 2.7 gated.2
  253.5 13.0 %all_to_all.28.parts_ref = bf16[4,40,2048]{2,1,0:T(8,128)(2,1)S(1)} all-to-all(bf16[4,40,2048]{2,1,0:T(8,128)(2,1)S(1)} %pair_sum.5), channel_id=1, replica_groups={{0,2,4,6},{1,3,5,7},{8,10,12,14},{9,11,13,15},{16,18,20,22},{17,19,21,2..., dimensions={0} | all-to-all | bytes 1310720 | tf_op jit(solution)/shard_map/all_to_all | solution.py:408
  (181 shorter events, 90.5 us)
Async XLA Ops:
  13.7 19.2 %collective-permute-start.8 = (bf16[160,1408]{1,0:T(8,128)(2,1)S(1)}, bf16[160,1408]{1,0:T(8,128)(2,1)S(1)}, u32[]{:S(2)}, u32[]{:S(2)}) collective-permute-start(bf16[160,1408]{1,0:T(8,128)(2,1)S(1)} %constant_dynamic-update-slice_fusion.refs_0_.refs_8_), channel_id=1, source_target_pairs={{0,480},{8,488},{16,496},{24,504},{32,0},{40,8},{48,16},{56,24},{6... | collective-permute-start | bytes 1351688 | tf_op jit(solution)/shard_map/ppermute | solution.py:35
  25.9 12.4 %collective-permute-start = (bf16[160,1408]{1,0:T(8,128)(2,1)S(1)}, bf16[160,1408]{1,0:T(8,128)(2,1)S(1)}, u32[]{:S(2)}, u32[]{:S(2)}) collective-permute-start(bf16[160,1408]{1,0:T(8,128)(2,1)S(1)} %constant_dynamic-update-slice_fusion.refs_0_.refs_8_), channel_id=1, source_target_pairs={{0,32},{8,40},{16,48},{24,56},{32,64},{40,72},{48,80},{56,88},{64,... | collective-permute-start | bytes 1351688 | tf_op jit(solution)/shard_map/ppermute | solution.py:35
  33.0 11.6 %collective-permute-start.9 = (bf16[160,1408]{1,0:T(8,128)(2,1)S(1)}, bf16[160,1408]{1,0:T(8,128)(2,1)S(1)}, u32[]{:S(2)}, u32[]{:S(2)}) collective-permute-start(bf16[160,1408]{1,0:T(8,128)(2,1)S(1)} %collective-permute-done.8.refs_2_.refs_9_), channel_id=1, source_target_pairs={{0,480},{8,488},{16,496},{24,504},{32,0},{40,8},{48,16},{56,24},{6... | collective-permute-start | bytes 1351688 | tf_op jit(solution)/shard_map/ppermute | solution.py:35
  38.3 11.5 %collective-permute-start.1 = (bf16[160,1408]{1,0:T(8,128)(2,1)S(1)}, bf16[160,1408]{1,0:T(8,128)(2,1)S(1)}, u32[]{:S(2)}, u32[]{:S(2)}) collective-permute-start(bf16[160,1408]{1,0:T(8,128)(2,1)S(1)} %collective-permute-done.refs_1_.refs_7_), channel_id=1, source_target_pairs={{0,32},{8,40},{16,48},{24,56},{32,64},{40,72},{48,80},{56,88},{64,... | collective-permute-start | bytes 1351688 | tf_op jit(solution)/shard_map/ppermute | solution.py:35
  44.5 10.6 %collective-permute-start.10 = (bf16[160,1408]{1,0:T(8,128)(2,1)S(1)}, bf16[160,1408]{1,0:T(8,128)(2,1)S(1)}, u32[]{:S(2)}, u32[]{:S(2)}) collective-permute-start(bf16[160,1408]{1,0:T(8,128)(2,1)S(1)} %collective-permute-done.9.refs_1_.refs_10_), channel_id=1, source_target_pairs={{0,480},{8,488},{16,496},{24,504},{32,0},{40,8},{48,16},{56,24},{6... | collective-permute-start | bytes 1351688 | tf_op jit(solution)/shard_map/ppermute | solution.py:35
  49.9 10.7 %collective-permute-start.2 = (bf16[160,1408]{1,0:T(8,128)(2,1)S(1)}, bf16[160,1408]{1,0:T(8,128)(2,1)S(1)}, u32[]{:S(2)}, u32[]{:S(2)}) collective-permute-start(bf16[160,1408]{1,0:T(8,128)(2,1)S(1)} %collective-permute-done.1.refs_0_.refs_6_), channel_id=1, source_target_pairs={{0,32},{8,40},{16,48},{24,56},{32,64},{40,72},{48,80},{56,88},{64,... | collective-permute-start | bytes 1351688 | tf_op jit(solution)/shard_map/ppermute | solution.py:35
  55.2 10.7 %collective-permute-start.11 = (bf16[160,1408]{1,0:T(8,128)(2,1)S(1)}, bf16[160,1408]{1,0:T(8,128)(2,1)S(1)}, u32[]{:S(2)}, u32[]{:S(2)}) collective-permute-start(bf16[160,1408]{1,0:T(8,128)(2,1)S(1)} %collective-permute-done.10.refs_1_.refs_11_), channel_id=1, source_target_pairs={{0,480},{8,488},{16,496},{24,504},{32,0},{40,8},{48,16},{56,24},{6... | collective-permute-start | bytes 1351688 | tf_op jit(solution)/shard_map/ppermute | solution.py:35
  60.6 10.3 %collective-permute-start.3 = (bf16[160,1408]{1,0:T(8,128)(2,1)S(1)}, bf16[160,1408]{1,0:T(8,128)(2,1)S(1)}, u32[]{:S(2)}, u32[]{:S(2)}) collective-permute-start(bf16[160,1408]{1,0:T(8,128)(2,1)S(1)} %collective-permute-done.2.refs_0_.refs_5_), channel_id=1, source_target_pairs={{0,32},{8,40},{16,48},{24,56},{32,64},{40,72},{48,80},{56,88},{64,... | collective-permute-start | bytes 1351688 | tf_op jit(solution)/shard_map/ppermute | solution.py:35
  65.9 10.4 %collective-permute-start.12 = (bf16[160,1408]{1,0:T(8,128)(2,1)S(1)}, bf16[160,1408]{1,0:T(8,128)(2,1)S(1)}, u32[]{:S(2)}, u32[]{:S(2)}) collective-permute-start(bf16[160,1408]{1,0:T(8,128)(2,1)S(1)} %collective-permute-done.11.refs_1_.refs_12_), channel_id=1, source_target_pairs={{0,480},{8,488},{16,496},{24,504},{32,0},{40,8},{48,16},{56,24},{6... | collective-permute-start | bytes 1351688 | tf_op jit(solution)/shard_map/ppermute | solution.py:35
  70.9 10.7 %collective-permute-start.4 = (bf16[160,1408]{1,0:T(8,128)(2,1)S(1)}, bf16[160,1408]{1,0:T(8,128)(2,1)S(1)}, u32[]{:S(2)}, u32[]{:S(2)}) collective-permute-start(bf16[160,1408]{1,0:T(8,128)(2,1)S(1)} %collective-permute-done.3.refs_0_.refs_4_), channel_id=1, source_target_pairs={{0,32},{8,40},{16,48},{24,56},{32,64},{40,72},{48,80},{56,88},{64,... | collective-permute-start | bytes 1351688 | tf_op jit(solution)/shard_map/ppermute | solution.py:35
  76.3 17.9 %collective-permute-start.13 = (bf16[160,1408]{1,0:T(8,128)(2,1)S(1)}, bf16[160,1408]{1,0:T(8,128)(2,1)S(1)}, u32[]{:S(2)}, u32[]{:S(2)}) collective-permute-start(bf16[160,1408]{1,0:T(8,128)(2,1)S(1)} %collective-permute-done.12.refs_1_.refs_13_), channel_id=1, source_target_pairs={{0,480},{8,488},{16,496},{24,504},{32,0},{40,8},{48,16},{56,24},{6... | collective-permute-start | bytes 1351688 | tf_op jit(solution)/shard_map/ppermute | solution.py:35
  81.6 17.2 %collective-permute-start.5 = (bf16[160,1408]{1,0:T(8,128)(2,1)S(1)}, bf16[160,1408]{1,0:T(8,128)(2,1)S(1)}, u32[]{:S(2)}, u32[]{:S(2)}) collective-permute-start(bf16[160,1408]{1,0:T(8,128)(2,1)S(1)} %collective-permute-done.4.refs_0_.refs_3_), channel_id=1, source_target_pairs={{0,32},{8,40},{16,48},{24,56},{32,64},{40,72},{48,80},{56,88},{64,... | collective-permute-start | bytes 1351688 | tf_op jit(solution)/shard_map/ppermute | solution.py:35
  86.4 35.5 %collective-permute-start.17 = (bf16[352,960]{1,0:T(8,128)(2,1)}, bf16[352,960]{1,0:T(8,128)(2,1)S(1)}, u32[]{:S(2)}, u32[]{:S(2)}) collective-permute-start(bf16[352,960]{1,0:T(8,128)(2,1)} %slice_dynamic-update-slice_fusion.3.refs_0_), channel_id=1, source_target_pairs={{0,24},{8,0},{16,8},{24,16},{32,56},{40,32},{48,40},{56,48},{64,88... | collective-permute-start | bytes 2027528 | tf_op jit(solution)/shard_map/ppermute | solution.py:35
  89.7 35.8 %collective-permute-start.16 = (bf16[352,960]{1,0:T(8,128)(2,1)}, bf16[352,960]{1,0:T(8,128)(2,1)S(1)}, u32[]{:S(2)}, u32[]{:S(2)}) collective-permute-start(bf16[352,960]{1,0:T(8,128)(2,1)} %slice_dynamic-update-slice_fusion.3.refs_0_), channel_id=1, source_target_pairs={{0,16},{8,24},{16,0},{24,8},{32,48},{40,56},{48,32},{56,40},{64,80... | collective-permute-start | bytes 2027528 | tf_op jit(solution)/shard_map/ppermute | solution.py:35
  92.2 46.2 %collective-permute-start.15 = (bf16[352,960]{1,0:T(8,128)(2,1)}, bf16[352,960]{1,0:T(8,128)(2,1)}, u32[]{:S(2)}, u32[]{:S(2)}) collective-permute-start(bf16[352,960]{1,0:T(8,128)(2,1)} %slice_dynamic-update-slice_fusion.3.refs_0_), channel_id=1, source_target_pairs={{0,8},{8,16},{16,24},{24,0},{32,40},{40,48},{48,56},{56,32},{64,72... | collective-permute-start | bytes 2027528 | tf_op jit(solution)/shard_map/ppermute | solution.py:35
  94.2 18.4 %collective-permute-start.14 = (bf16[160,1408]{1,0:T(8,128)(2,1)S(1)}, bf16[160,1408]{1,0:T(8,128)(2,1)S(1)}, u32[]{:S(2)}, u32[]{:S(2)}) collective-permute-start(bf16[160,1408]{1,0:T(8,128)(2,1)S(1)} %collective-permute-done.13.refs_1_.refs_14_), channel_id=1, source_target_pairs={{0,480},{8,488},{16,496},{24,504},{32,0},{40,8},{48,16},{56,24},{6... | collective-permute-start | bytes 1351688 | tf_op jit(solution)/shard_map/ppermute | solution.py:35
  98.8 10.5 %collective-permute-start.6 = (bf16[160,1408]{1,0:T(8,128)(2,1)S(1)}, bf16[160,1408]{1,0:T(8,128)(2,1)}, u32[]{:S(2)}, u32[]{:S(2)}) collective-permute-start(bf16[160,1408]{1,0:T(8,128)(2,1)S(1)} %collective-permute-done.5.refs_0_.refs_2_), channel_id=1, source_target_pairs={{0,32},{8,40},{16,48},{24,56},{32,64},{40,72},{48,80},{56,88},{64,... | collective-permute-start | bytes 1351688 | tf_op jit(solution)/shard_map/ppermute | solution.py:35
  109.3 7.4 %collective-permute-start.18 = (bf16[32,960]{1,0:T(8,128)(2,1)S(1)}, bf16[32,960]{1,0:T(8,128)(2,1)S(1)}, u32[]{:S(2)}, u32[]{:S(2)}) collective-permute-start(bf16[32,960]{1,0:T(8,128)(2,1)S(1)} %get-tuple-element.37), channel_id=1, source_target_pairs={{0,64},{8,72},{16,80},{24,88},{32,96},{40,104},{48,112},{56,120},{... | collective-permute-start | bytes 184328 | tf_op jit(solution)/shard_map/ppermute | solution.py:35
  112.7 27.8 %collective-permute-start.7 = (bf16[160,1408]{1,0:T(8,128)(2,1)}, bf16[160,1408]{1,0:T(8,128)(2,1)}, u32[]{:S(2)}, u32[]{:S(2)}) collective-permute-start(bf16[160,1408]{1,0:T(8,128)(2,1)} %collective-permute-done.6.refs_0_.refs_1_), channel_id=1, source_target_pairs={{0,32},{8,40},{16,48},{24,56},{32,64},{40,72},{48,80},{56,88},{64,... | collective-permute-start | bytes 1351688 | tf_op jit(solution)/shard_map/ppermute | solution.py:35
  117.3 21.1 %collective-permute-start.21 = (bf16[160,960]{1,0:T(8,128)(2,1)}, bf16[160,960]{1,0:T(8,128)(2,1)}, u32[]{:S(2)}, u32[]{:S(2)}) collective-permute-start(bf16[160,960]{1,0:T(8,128)(2,1)} %constant_dynamic-update-slice_fusion.2.refs_4_), channel_id=1, source_target_pairs={{0,24},{8,0},{16,8},{24,16},{32,56},{40,32},{48,40},{56,48},{64,88... | collective-permute-start | bytes 921608 | tf_op jit(solution)/shard_map/ppermute | solution.py:35
  122.9 15.6 %collective-permute-start.20 = (bf16[160,960]{1,0:T(8,128)(2,1)}, bf16[160,960]{1,0:T(8,128)(2,1)}, u32[]{:S(2)}, u32[]{:S(2)}) collective-permute-start(bf16[160,960]{1,0:T(8,128)(2,1)} %constant_dynamic-update-slice_fusion.2.refs_4_), channel_id=1, source_target_pairs={{0,16},{8,24},{16,0},{24,8},{32,48},{40,56},{48,32},{56,40},{64,80... | collective-permute-start | bytes 921608 | tf_op jit(solution)/shard_map/ppermute | solution.py:35
  126.3 12.1 %collective-permute-start.19 = (bf16[160,960]{1,0:T(8,128)(2,1)}, bf16[160,960]{1,0:T(8,128)(2,1)}, u32[]{:S(2)}, u32[]{:S(2)}) collective-permute-start(bf16[160,960]{1,0:T(8,128)(2,1)} %constant_dynamic-update-slice_fusion.2.refs_4_), channel_id=1, source_target_pairs={{0,8},{8,16},{16,24},{24,0},{32,40},{40,48},{48,56},{56,32},{64,72... | collective-permute-start | bytes 921608 | tf_op jit(solution)/shard_map/ppermute | solution.py:35
  143.8 24.9 %collective-permute-start.22 = (bf16[160,2048]{1,0:T(8,128)(2,1)S(1)}, bf16[160,2048]{1,0:T(8,128)(2,1)S(1)}, u32[]{:S(2)}, u32[]{:S(2)}) collective-permute-start(bf16[160,2048]{1,0:T(8,128)(2,1)S(1)} %down.5), channel_id=1, source_target_pairs={{0,1},{1,0},{2,3},{3,2},{4,5},{5,4},{6,7},{7,6},{8,9},{9,8},{10,11... | collective-permute-start | bytes 1966088 | tf_op jit(solution)/shard_map/ppermute | solution.py:403
  169.8 14.7 %all-to-all-start = ((bf16[4,40,2048]{2,1,0:T(8,128)(2,1)}), bf16[4,40,2048]{2,1,0:T(8,128)(2,1)}, u32[]{:S(2)}, u32[]{:S(2)}) async-start(bf16[4,40,2048]{2,1,0:T(8,128)(2,1)} %copy-done.2), calls=%async_computation | async-start | bytes 1310720 | tf_op jit(solution)/shard_map/all_to_all | solution.py:408
  (52 other events, 1197.6 us)
where the time goes:
time: 269 us; the launch traced here: 267 us
  starting transfers between devices  117 us (43%)
  blocking collectives  62 us (23%)
  waiting for transfers between devices  32.7 us (12%)
  local copies, waits for them, and re-layouts  27.8 us (10%)
  Pallas kernels  26.6 us (10%)
    ppermute x22, starting transfers between devices, shift(): return lax.ppermute(array, 'fs', fs_shift(dy, dz))  77 us
    ppermute x5, starting transfers between devices, core_swap(): return lax.ppermute(array, 'tp', [(k, k ^ 1) for k in range(8)])  35.9 us
    all_to_all x2, blocking collectives, shares_of_rows(): lax.all_to_all(tiles, 'tp', 0, 0, tiled=True, axis_index_groups=X_GROUPS)  26.3 us
    all_to_all x2, blocking collectives, rows_of_all(): lax.all_to_all(copies, 'tp', 0, 0, tiled=True, axis_index_groups=X_GROUPS)  24.6 us
    unnamed x110, local copies, waits for them, and re-layouts  24.1 us
    ppermute x22, waiting for transfers between devices, shift(): return lax.ppermute(array, 'fs', fs_shift(dy, dz))  18.2 us
    all_gather x1, blocking collectives, body(): lax.all_gather(first, 'fs', axis=0, tiled=True, axis_index_groups=groups)  11.1 us
    all_to_all x1, waiting for transfers between devices, shares_of_rows(): lax.all_to_all(tiles, 'tp', 0, 0, tiled=True, axis_index_groups=X_GROUPS)  9.42 us
  transfers between devices with their start and end apart: 28, of which 13 were waited for; matrix products, arithmetic and copies ran while one was open for 5% of the time, Pallas kernels for 5%

commit v1 on v0

--- a/solution.py
+++ b/solution.py
@@ -346,13 +346,30 @@
     )(a, b)
 
 
+def pooled_kernel(x_ref, w_ref, out_ref):
+    out_ref[...] = jnp.dot(x_ref[...], w_ref[:, 0:128], preferred_element_type=F32).astype(BF)
+
+
+def pooled(x, w):
+    return pl.pallas_call(
+        pooled_kernel,
+        out_shape=jax.ShapeDtypeStruct((x.shape[0], 128), BF),
+        in_specs=[VMEM] * 2,
+        out_specs=VMEM,
+        compiler_params=limit(6),
+        cost_estimate=pl.CostEstimate(
+            flops=2 * x.shape[0] * x.shape[1] * 128, bytes_accessed=2 << 20, transcendentals=0
+        ),
+        name="pooled",
+    )(x, w)
+
+
 def mixer_kernel(kind_ref, mine_ref, other_ref, w_ref, pool_ref, scale_ref, keep_ref, send_ref):
     rows = 2 * mine_ref.shape[0]
     tile = rows // 8
     kind, core = kind_ref[0], kind_ref[1]
-    x = jnp.concatenate([mine_ref[...], other_ref[...]], axis=0)
-    values = jnp.dot(x, w_ref[:, 0:128], preferred_element_type=F32)
-    values = values.astype(BF).astype(F32)
+    values = jnp.dot(other_ref[...], w_ref[:, 0:128], preferred_element_type=F32).astype(BF)
+    values = jnp.concatenate([mine_ref[...].astype(F32), values.astype(F32)], axis=0)
     in_order = []
     for i in range(4):
         mine = values[i * tile : (i + 1) * tile]
@@ -382,7 +399,7 @@
 
 
 def mixer(kind, mine, other, w, pool_w, pool_scale):
-    rows, depth = 2 * mine.shape[0], mine.shape[1]
+    rows, depth = 2 * other.shape[0], other.shape[1]
     return pl.pallas_call(
         mixer_kernel,
         out_shape=(jax.ShapeDtypeStruct((rows // 2, depth), BF),) * 2,
@@ -460,7 +477,8 @@
     parts = shares_of_rows(mine, other)
     stream, copies = settle(parts, stream, gains, 1, 0.5)
     kind = jnp.stack([numbers[2], numbers[1]])
-    share = mixer(kind, *rows_of_all(copies), mix_w, pool_w[0], pool_scale[None])
+    mine, other = rows_of_all(copies)
+    share = mixer(kind, pooled(mine, mix_w), other, mix_w, pool_w[0], pool_scale[None])
     stream, copies = settle(shares_of_rows(*share), stream, gains, 3, 1.0)
     mine, other = rows_of_all(copies)
     hidden, gate_up = gated(mine, payloads, width)

time: 269 us -> 268 us (level)
    unnamed x110 -> x112, local copies, waits for them, and re-layouts: 24.1 us -> 24 us
  transfers between devices with their start and end apart: 28 -> 28, of which waited for: 13 -> 12; matrix products, arithmetic and copies ran while one was open for 5% -> 5% of each run, Pallas kernels for 5% -> 5%
where the time goes in v1:
time: 268 us; the launch traced here: 266 us
  starting transfers between devices  117 us (44%)
  blocking collectives  62.2 us (23%)
  waiting for transfers between devices  31.2 us (12%)
  local copies, waits for them, and re-layouts  27.7 us (10%)
  Pallas kernels  27.1 us (10%)
    ppermute x22, starting transfers between devices, shift(): return lax.ppermute(array, 'fs', fs_shift(dy, dz))  77 us
    ppermute x5, starting transfers between devices, core_swap(): return lax.ppermute(array, 'tp', [(k, k ^ 1) for k in range(8)])  35.5 us
    all_to_all x2, blocking collectives, shares_of_rows(): lax.all_to_all(tiles, 'tp', 0, 0, tiled=True, axis_index_groups=X_GROUPS)  26.3 us
    all_to_all x2, blocking collectives, rows_of_all(): lax.all_to_all(copies, 'tp', 0, 0, tiled=True, axis_index_groups=X_GROUPS)  24.8 us
    unnamed x112, local copies, waits for them, and re-layouts  24 us
    ppermute x22, waiting for transfers between devices, shift(): return lax.ppermute(array, 'fs', fs_shift(dy, dz))  18.3 us
    all_gather x1, blocking collectives, body(): lax.all_gather(first, 'fs', axis=0, tiled=True, axis_index_groups=groups)  11.1 us
    all_to_all x1, waiting for transfers between devices, shares_of_rows(): lax.all_to_all(tiles, 'tp', 0, 0, tiled=True, axis_index_groups=X_GROUPS)  9.41 us
  transfers between devices with their start and end apart: 28, of which 12 were waited for; matrix products, arithmetic and copies ran while one was open for 5% of the time, Pallas kernels for 5%

profile of v1, /device:TPU:1, one launch (start us, length us, event | category | flops | bytes accessed | tf_op | source)
XLA Modules:
  0.0 266.1 jit_solution(2195320165860442380)
XLA Ops:
  1.7 11.1 %all_gather.3 = bf16[128,1408]{1,0:T(8,128)(2,1)S(1)} all-gather(bf16[32,1408]{1,0:T(8,128)(2,1)} %get-tuple-element.21), channel_id=1, replica_groups={{0,8,16,24},{32,40,48,56},{64,72,80,88},{96,104,112,120},{128,136,144,1..., dimensions={0}, use_global_device_ids=true | all-gather | bytes 450560 | tf_op jit(solution)/shard_map/all_gather | solution.py:444
  13.7 12.1 %collective-permute-start.8 = (bf16[160,1408]{1,0:T(8,128)(2,1)S(1)}, bf16[160,1408]{1,0:T(8,128)(2,1)S(1)}, u32[]{:S(2)}, u32[]{:S(2)}) collective-permute-start(bf16[160,1408]{1,0:T(8,128)(2,1)S(1)} %constant_dynamic-update-slice_fusion.refs_0_.refs_8_), channel_id=1, source_target_pairs={{0,480},{8,488},{16,496},{24,504},{32,0},{40,8},{48,16},{56,24},{6... | collective-permute-start | bytes 1351688 | tf_op jit(solution)/shard_map/ppermute | solution.py:35
  29.4 3.6 %collective-permute-done.8.refs_2_.refs_9_ = bf16[160,1408]{1,0:T(8,128)(2,1)S(1)} collective-permute-done((bf16[160,1408]{1,0:T(8,128)(2,1)S(1)}, bf16[160,1408]{1,0:T(8,128)(2,1)S(1)}, u32[]{:S(2)}, u32[]{:S(2)}) %collective-permute-start.8) | collective-permute-done | bytes 450592 | tf_op jit(solution)/shard_map/ppermute | solution.py:35
  33.0 5.3 %collective-permute-start.9 = (bf16[160,1408]{1,0:T(8,128)(2,1)S(1)}, bf16[160,1408]{1,0:T(8,128)(2,1)S(1)}, u32[]{:S(2)}, u32[]{:S(2)}) collective-permute-start(bf16[160,1408]{1,0:T(8,128)(2,1)S(1)} %collective-permute-done.8.refs_2_.refs_9_), channel_id=1, source_target_pairs={{0,480},{8,488},{16,496},{24,504},{32,0},{40,8},{48,16},{56,24},{6... | collective-permute-start | bytes 1351688 | tf_op jit(solution)/shard_map/ppermute | solution.py:35
  41.5 3.0 %collective-permute-done.9.refs_1_.refs_10_ = bf16[160,1408]{1,0:T(8,128)(2,1)S(1)} collective-permute-done((bf16[160,1408]{1,0:T(8,128)(2,1)S(1)}, bf16[160,1408]{1,0:T(8,128)(2,1)S(1)}, u32[]{:S(2)}, u32[]{:S(2)}) %collective-permute-start.9) | collective-permute-done | bytes 450592 | tf_op jit(solution)/shard_map/ppermute | solution.py:35
  44.5 5.3 %collective-permute-start.10 = (bf16[160,1408]{1,0:T(8,128)(2,1)S(1)}, bf16[160,1408]{1,0:T(8,128)(2,1)S(1)}, u32[]{:S(2)}, u32[]{:S(2)}) collective-permute-start(bf16[160,1408]{1,0:T(8,128)(2,1)S(1)} %collective-permute-done.9.refs_1_.refs_10_), channel_id=1, source_target_pairs={{0,480},{8,488},{16,496},{24,504},{32,0},{40,8},{48,16},{56,24},{6... | collective-permute-start | bytes 1351688 | tf_op jit(solution)/shard_map/ppermute | solution.py:35
  55.2 5.4 %collective-permute-start.11 = (bf16[160,1408]{1,0:T(8,128)(2,1)S(1)}, bf16[160,1408]{1,0:T(8,128)(2,1)S(1)}, u32[]{:S(2)}, u32[]{:S(2)}) collective-permute-start(bf16[160,1408]{1,0:T(8,128)(2,1)S(1)} %collective-permute-done.10.refs_1_.refs_11_), channel_id=1, source_target_pairs={{0,480},{8,488},{16,496},{24,504},{32,0},{40,8},{48,16},{56,24},{6... | collective-permute-start | bytes 1351688 | tf_op jit(solution)/shard_map/ppermute | solution.py:35
  65.9 5.0 %collective-permute-start.12 = (bf16[160,1408]{1,0:T(8,128)(2,1)S(1)}, bf16[160,1408]{1,0:T(8,128)(2,1)S(1)}, u32[]{:S(2)}, u32[]{:S(2)}) collective-permute-start(bf16[160,1408]{1,0:T(8,128)(2,1)S(1)} %collective-permute-done.11.refs_1_.refs_12_), channel_id=1, source_target_pairs={{0,480},{8,488},{16,496},{24,504},{32,0},{40,8},{48,16},{56,24},{6... | collective-permute-start | bytes 1351688 | tf_op jit(solution)/shard_map/ppermute | solution.py:35
  76.3 5.0 %collective-permute-start.13 = (bf16[160,1408]{1,0:T(8,128)(2,1)S(1)}, bf16[160,1408]{1,0:T(8,128)(2,1)S(1)}, u32[]{:S(2)}, u32[]{:S(2)}) collective-permute-start(bf16[160,1408]{1,0:T(8,128)(2,1)S(1)} %collective-permute-done.12.refs_1_.refs_13_), channel_id=1, source_target_pairs={{0,480},{8,488},{16,496},{24,504},{32,0},{40,8},{48,16},{56,24},{6... | collective-permute-start | bytes 1351688 | tf_op jit(solution)/shard_map/ppermute | solution.py:35
  86.4 3.3 %collective-permute-start.17 = (bf16[352,960]{1,0:T(8,128)(2,1)}, bf16[352,960]{1,0:T(8,128)(2,1)S(1)}, u32[]{:S(2)}, u32[]{:S(2)}) collective-permute-start(bf16[352,960]{1,0:T(8,128)(2,1)} %slice_dynamic-update-slice_fusion.3.refs_0_), channel_id=1, source_target_pairs={{0,24},{8,0},{16,8},{24,16},{32,56},{40,32},{48,40},{56,48},{64,88... | collective-permute-start | bytes 2027528 | tf_op jit(solution)/shard_map/ppermute | solution.py:35
  94.2 4.6 %collective-permute-start.14 = (bf16[160,1408]{1,0:T(8,128)(2,1)S(1)}, bf16[160,1408]{1,0:T(8,128)(2,1)S(1)}, u32[]{:S(2)}, u32[]{:S(2)}) collective-permute-start(bf16[160,1408]{1,0:T(8,128)(2,1)S(1)} %collective-permute-done.13.refs_1_.refs_14_), channel_id=1, source_target_pairs={{0,480},{8,488},{16,496},{24,504},{32,0},{40,8},{48,16},{56,24},{6... | collective-permute-start | bytes 1351688 | tf_op jit(solution)/shard_map/ppermute | solution.py:35
  103.5 5.7 %collective-permute-done.6.refs_0_.refs_1_ = bf16[160,1408]{1,0:T(8,128)(2,1)} collective-permute-done((bf16[160,1408]{1,0:T(8,128)(2,1)S(1)}, bf16[160,1408]{1,0:T(8,128)(2,1)}, u32[]{:S(2)}, u32[]{:S(2)}) %collective-permute-start.6) | collective-permute-done | bytes 450592 | tf_op jit(solution)/shard_map/ppermute | solution.py:35
  117.3 4.7 %collective-permute-start.21 = (bf16[160,960]{1,0:T(8,128)(2,1)}, bf16[160,960]{1,0:T(8,128)(2,1)}, u32[]{:S(2)}, u32[]{:S(2)}) collective-permute-start(bf16[160,960]{1,0:T(8,128)(2,1)} %constant_dynamic-update-slice_fusion.2.refs_4_), channel_id=1, source_target_pairs={{0,24},{8,0},{16,8},{24,16},{32,56},{40,32},{48,40},{56,48},{64,88... | collective-permute-start | bytes 921608 | tf_op jit(solution)/shard_map/ppermute | solution.py:35
  122.8 2.6 collective-permute-start.20
  143.8 23.2 %collective-permute-start.22 = (bf16[160,2048]{1,0:T(8,128)(2,1)S(1)}, bf16[160,2048]{1,0:T(8,128)(2,1)S(1)}, u32[]{:S(2)}, u32[]{:S(2)}) collective-permute-start(bf16[160,2048]{1,0:T(8,128)(2,1)S(1)} %down.5), channel_id=1, source_target_pairs={{0,1},{1,0},{2,3},{3,2},{4,5},{5,4},{6,7},{7,6},{8,9},{9,8},{10,11... | collective-permute-start | bytes 1966088 | tf_op jit(solution)/shard_map/ppermute | solution.py:420
  169.7 4.2 %all-to-all-start = ((bf16[4,40,2048]{2,1,0:T(8,128)(2,1)}), bf16[4,40,2048]{2,1,0:T(8,128)(2,1)}, u32[]{:S(2)}, u32[]{:S(2)}) async-start(bf16[4,40,2048]{2,1,0:T(8,128)(2,1)} %copy-done.5), calls=%async_computation | async-start | bytes 1310720 | tf_op jit(solution)/shard_map/all_to_all | solution.py:425
  175.0 9.4 %all-to-all-done.parts_ref = bf16[4,40,2048]{2,1,0:T(8,128)(2,1)} async-done(((bf16[4,40,2048]{2,1,0:T(8,128)(2,1)}), bf16[4,40,2048]{2,1,0:T(8,128)(2,1)}, u32[]{:S(2)}, u32[]{:S(2)}) %all-to-all-start) | async-done | bytes 655392 | tf_op jit(solution)/shard_map/all_to_all | solution.py:425
  185.8 12.4 %all_to_all.25 = bf16[4,40,2048]{2,1,0:T(8,128)(2,1)} all-to-all(bf16[4,40,2048]{2,1,0:T(8,128)(2,1)S(1)} %get-tuple-element.28), channel_id=1, replica_groups={{0,2,4,6},{1,3,5,7},{8,10,12,14},{9,11,13,15},{16,18,20,22},{17,19,21,2..., dimensions={0} | all-to-all | bytes 1310720 | tf_op jit(solution)/shard_map/all_to_all | solution.py:429
  198.2 4.4 %collective-permute-start.23 = (bf16[160,2048]{1,0:T(8,128)(2,1)}, bf16[160,2048]{1,0:T(8,128)(2,1)}, u32[]{:S(2)}, u32[]{:S(2)}) collective-permute-start(bf16[160,2048]{1,0:T(8,128)(2,1)} %bitcast.6.x_ref), channel_id=1, source_target_pairs={{0,1},{1,0},{2,3},{3,2},{4,5},{5,4},{6,7},{7,6},{8,9},{9,8},{10,11... | collective-permute-start | bytes 1966088 | tf_op jit(solution)/shard_map/ppermute | solution.py:420
  212.7 13.3 %all_to_all.26.parts_ref = bf16[4,40,2048]{2,1,0:T(8,128)(2,1)S(1)} all-to-all(bf16[4,40,2048]{2,1,0:T(8,128)(2,1)S(1)} %pair_sum.4), channel_id=1, replica_groups={{0,2,4,6},{1,3,5,7},{8,10,12,14},{9,11,13,15},{16,18,20,22},{17,19,21,2..., dimensions={0} | all-to-all | bytes 1310720 | tf_op jit(solution)/shard_map/all_to_all | solution.py:425
  226.3 12.4 %all_to_all.27 = bf16[4,40,2048]{2,1,0:T(8,128)(2,1)S(1)} all-to-all(bf16[4,40,2048]{2,1,0:T(8,128)(2,1)S(1)} %get-tuple-element.33), channel_id=1, replica_groups={{0,2,4,6},{1,3,5,7},{8,10,12,14},{9,11,13,15},{16,18,20,22},{17,19,21,2..., dimensions={0} | all-to-all | bytes 1310720 | tf_op jit(solution)/shard_map/all_to_all | solution.py:429
  238.6 4.0 %collective-permute-start.25 = (bf16[160,2048]{1,0:T(8,128)(2,1)S(1)}, bf16[160,2048]{1,0:T(8,128)(2,1)S(1)}, u32[]{:S(2)}, u32[]{:S(2)}) collective-permute-start(bf16[160,2048]{1,0:T(8,128)(2,1)S(1)} %bitcast.10), channel_id=1, source_target_pairs={{0,1},{1,0},{2,3},{3,2},{4,5},{5,4},{6,7},{7,6},{8,9},{9,8},{10,11... | collective-permute-start | bytes 1966088 | tf_op jit(solution)/shard_map/ppermute | solution.py:420
  242.8 2.7 gated.2
  252.2 13.0 %all_to_all.28.parts_ref = bf16[4,40,2048]{2,1,0:T(8,128)(2,1)S(1)} all-to-all(bf16[4,40,2048]{2,1,0:T(8,128)(2,1)S(1)} %pair_sum.5), channel_id=1, replica_groups={{0,2,4,6},{1,3,5,7},{8,10,12,14},{9,11,13,15},{16,18,20,22},{17,19,21,2..., dimensions={0} | all-to-all | bytes 1310720 | tf_op jit(solution)/shard_map/all_to_all | solution.py:425
  (184 shorter events, 89.5 us)
Async XLA Ops:
  13.7 19.2 %collective-permute-start.8 = (bf16[160,1408]{1,0:T(8,128)(2,1)S(1)}, bf16[160,1408]{1,0:T(8,128)(2,1)S(1)}, u32[]{:S(2)}, u32[]{:S(2)}) collective-permute-start(bf16[160,1408]{1,0:T(8,128)(2,1)S(1)} %constant_dynamic-update-slice_fusion.refs_0_.refs_8_), channel_id=1, source_target_pairs={{0,480},{8,488},{16,496},{24,504},{32,0},{40,8},{48,16},{56,24},{6... | collective-permute-start | bytes 1351688 | tf_op jit(solution)/shard_map/ppermute | solution.py:35
  25.9 12.4 %collective-permute-start = (bf16[160,1408]{1,0:T(8,128)(2,1)S(1)}, bf16[160,1408]{1,0:T(8,128)(2,1)S(1)}, u32[]{:S(2)}, u32[]{:S(2)}) collective-permute-start(bf16[160,1408]{1,0:T(8,128)(2,1)S(1)} %constant_dynamic-update-slice_fusion.refs_0_.refs_8_), channel_id=1, source_target_pairs={{0,32},{8,40},{16,48},{24,56},{32,64},{40,72},{48,80},{56,88},{64,... | collective-permute-start | bytes 1351688 | tf_op jit(solution)/shard_map/ppermute | solution.py:35
  33.0 11.6 %collective-permute-start.9 = (bf16[160,1408]{1,0:T(8,128)(2,1)S(1)}, bf16[160,1408]{1,0:T(8,128)(2,1)S(1)}, u32[]{:S(2)}, u32[]{:S(2)}) collective-permute-start(bf16[160,1408]{1,0:T(8,128)(2,1)S(1)} %collective-permute-done.8.refs_2_.refs_9_), channel_id=1, source_target_pairs={{0,480},{8,488},{16,496},{24,504},{32,0},{40,8},{48,16},{56,24},{6... | collective-permute-start | bytes 1351688 | tf_op jit(solution)/shard_map/ppermute | solution.py:35
  38.3 11.5 %collective-permute-start.1 = (bf16[160,1408]{1,0:T(8,128)(2,1)S(1)}, bf16[160,1408]{1,0:T(8,128)(2,1)S(1)}, u32[]{:S(2)}, u32[]{:S(2)}) collective-permute-start(bf16[160,1408]{1,0:T(8,128)(2,1)S(1)} %collective-permute-done.refs_1_.refs_7_), channel_id=1, source_target_pairs={{0,32},{8,40},{16,48},{24,56},{32,64},{40,72},{48,80},{56,88},{64,... | collective-permute-start | bytes 1351688 | tf_op jit(solution)/shard_map/ppermute | solution.py:35
  44.5 10.6 %collective-permute-start.10 = (bf16[160,1408]{1,0:T(8,128)(2,1)S(1)}, bf16[160,1408]{1,0:T(8,128)(2,1)S(1)}, u32[]{:S(2)}, u32[]{:S(2)}) collective-permute-start(bf16[160,1408]{1,0:T(8,128)(2,1)S(1)} %collective-permute-done.9.refs_1_.refs_10_), channel_id=1, source_target_pairs={{0,480},{8,488},{16,496},{24,504},{32,0},{40,8},{48,16},{56,24},{6... | collective-permute-start | bytes 1351688 | tf_op jit(solution)/shard_map/ppermute | solution.py:35
  49.9 10.7 %collective-permute-start.2 = (bf16[160,1408]{1,0:T(8,128)(2,1)S(1)}, bf16[160,1408]{1,0:T(8,128)(2,1)S(1)}, u32[]{:S(2)}, u32[]{:S(2)}) collective-permute-start(bf16[160,1408]{1,0:T(8,128)(2,1)S(1)} %collective-permute-done.1.refs_0_.refs_6_), channel_id=1, source_target_pairs={{0,32},{8,40},{16,48},{24,56},{32,64},{40,72},{48,80},{56,88},{64,... | collective-permute-start | bytes 1351688 | tf_op jit(solution)/shard_map/ppermute | solution.py:35
  55.2 10.7 %collective-permute-start.11 = (bf16[160,1408]{1,0:T(8,128)(2,1)S(1)}, bf16[160,1408]{1,0:T(8,128)(2,1)S(1)}, u32[]{:S(2)}, u32[]{:S(2)}) collective-permute-start(bf16[160,1408]{1,0:T(8,128)(2,1)S(1)} %collective-permute-done.10.refs_1_.refs_11_), channel_id=1, source_target_pairs={{0,480},{8,488},{16,496},{24,504},{32,0},{40,8},{48,16},{56,24},{6... | collective-permute-start | bytes 1351688 | tf_op jit(solution)/shard_map/ppermute | solution.py:35
  60.6 10.3 %collective-permute-start.3 = (bf16[160,1408]{1,0:T(8,128)(2,1)S(1)}, bf16[160,1408]{1,0:T(8,128)(2,1)S(1)}, u32[]{:S(2)}, u32[]{:S(2)}) collective-permute-start(bf16[160,1408]{1,0:T(8,128)(2,1)S(1)} %collective-permute-done.2.refs_0_.refs_5_), channel_id=1, source_target_pairs={{0,32},{8,40},{16,48},{24,56},{32,64},{40,72},{48,80},{56,88},{64,... | collective-permute-start | bytes 1351688 | tf_op jit(solution)/shard_map/ppermute | solution.py:35
  65.9 10.4 %collective-permute-start.12 = (bf16[160,1408]{1,0:T(8,128)(2,1)S(1)}, bf16[160,1408]{1,0:T(8,128)(2,1)S(1)}, u32[]{:S(2)}, u32[]{:S(2)}) collective-permute-start(bf16[160,1408]{1,0:T(8,128)(2,1)S(1)} %collective-permute-done.11.refs_1_.refs_12_), channel_id=1, source_target_pairs={{0,480},{8,488},{16,496},{24,504},{32,0},{40,8},{48,16},{56,24},{6... | collective-permute-start | bytes 1351688 | tf_op jit(solution)/shard_map/ppermute | solution.py:35
  70.9 10.7 %collective-permute-start.4 = (bf16[160,1408]{1,0:T(8,128)(2,1)S(1)}, bf16[160,1408]{1,0:T(8,128)(2,1)S(1)}, u32[]{:S(2)}, u32[]{:S(2)}) collective-permute-start(bf16[160,1408]{1,0:T(8,128)(2,1)S(1)} %collective-permute-done.3.refs_0_.refs_4_), channel_id=1, source_target_pairs={{0,32},{8,40},{16,48},{24,56},{32,64},{40,72},{48,80},{56,88},{64,... | collective-permute-start | bytes 1351688 | tf_op jit(solution)/shard_map/ppermute | solution.py:35
  76.3 17.9 %collective-permute-start.13 = (bf16[160,1408]{1,0:T(8,128)(2,1)S(1)}, bf16[160,1408]{1,0:T(8,128)(2,1)S(1)}, u32[]{:S(2)}, u32[]{:S(2)}) collective-permute-start(bf16[160,1408]{1,0:T(8,128)(2,1)S(1)} %collective-permute-done.12.refs_1_.refs_13_), channel_id=1, source_target_pairs={{0,480},{8,488},{16,496},{24,504},{32,0},{40,8},{48,16},{56,24},{6... | collective-permute-start | bytes 1351688 | tf_op jit(solution)/shard_map/ppermute | solution.py:35
  81.6 17.2 %collective-permute-start.5 = (bf16[160,1408]{1,0:T(8,128)(2,1)S(1)}, bf16[160,1408]{1,0:T(8,128)(2,1)S(1)}, u32[]{:S(2)}, u32[]{:S(2)}) collective-permute-start(bf16[160,1408]{1,0:T(8,128)(2,1)S(1)} %collective-permute-done.4.refs_0_.refs_3_), channel_id=1, source_target_pairs={{0,32},{8,40},{16,48},{24,56},{32,64},{40,72},{48,80},{56,88},{64,... | collective-permute-start | bytes 1351688 | tf_op jit(solution)/shard_map/ppermute | solution.py:35
  86.4 35.5 %collective-permute-start.17 = (bf16[352,960]{1,0:T(8,128)(2,1)}, bf16[352,960]{1,0:T(8,128)(2,1)S(1)}, u32[]{:S(2)}, u32[]{:S(2)}) collective-permute-start(bf16[352,960]{1,0:T(8,128)(2,1)} %slice_dynamic-update-slice_fusion.3.refs_0_), channel_id=1, source_target_pairs={{0,24},{8,0},{16,8},{24,16},{32,56},{40,32},{48,40},{56,48},{64,88... | collective-permute-start | bytes 2027528 | tf_op jit(solution)/shard_map/ppermute | solution.py:35
  89.7 35.8 %collective-permute-start.16 = (bf16[352,960]{1,0:T(8,128)(2,1)}, bf16[352,960]{1,0:T(8,128)(2,1)S(1)}, u32[]{:S(2)}, u32[]{:S(2)}) collective-permute-start(bf16[352,960]{1,0:T(8,128)(2,1)} %slice_dynamic-update-slice_fusion.3.refs_0_), channel_id=1, source_target_pairs={{0,16},{8,24},{16,0},{24,8},{32,48},{40,56},{48,32},{56,40},{64,80... | collective-permute-start | bytes 2027528 | tf_op jit(solution)/shard_map/ppermute | solution.py:35
  92.2 46.2 %collective-permute-start.15 = (bf16[352,960]{1,0:T(8,128)(2,1)}, bf16[352,960]{1,0:T(8,128)(2,1)}, u32[]{:S(2)}, u32[]{:S(2)}) collective-permute-start(bf16[352,960]{1,0:T(8,128)(2,1)} %slice_dynamic-update-slice_fusion.3.refs_0_), channel_id=1, source_target_pairs={{0,8},{8,16},{16,24},{24,0},{32,40},{40,48},{48,56},{56,32},{64,72... | collective-permute-start | bytes 2027528 | tf_op jit(solution)/shard_map/ppermute | solution.py:35
  94.2 18.4 %collective-permute-start.14 = (bf16[160,1408]{1,0:T(8,128)(2,1)S(1)}, bf16[160,1408]{1,0:T(8,128)(2,1)S(1)}, u32[]{:S(2)}, u32[]{:S(2)}) collective-permute-start(bf16[160,1408]{1,0:T(8,128)(2,1)S(1)} %collective-permute-done.13.refs_1_.refs_14_), channel_id=1, source_target_pairs={{0,480},{8,488},{16,496},{24,504},{32,0},{40,8},{48,16},{56,24},{6... | collective-permute-start | bytes 1351688 | tf_op jit(solution)/shard_map/ppermute | solution.py:35
  98.8 10.5 %collective-permute-start.6 = (bf16[160,1408]{1,0:T(8,128)(2,1)S(1)}, bf16[160,1408]{1,0:T(8,128)(2,1)}, u32[]{:S(2)}, u32[]{:S(2)}) collective-permute-start(bf16[160,1408]{1,0:T(8,128)(2,1)S(1)} %collective-permute-done.5.refs_0_.refs_2_), channel_id=1, source_target_pairs={{0,32},{8,40},{16,48},{24,56},{32,64},{40,72},{48,80},{56,88},{64,... | collective-permute-start | bytes 1351688 | tf_op jit(solution)/shard_map/ppermute | solution.py:35
  109.2 7.4 %collective-permute-start.18 = (bf16[32,960]{1,0:T(8,128)(2,1)S(1)}, bf16[32,960]{1,0:T(8,128)(2,1)S(1)}, u32[]{:S(2)}, u32[]{:S(2)}) collective-permute-start(bf16[32,960]{1,0:T(8,128)(2,1)S(1)} %get-tuple-element.37), channel_id=1, source_target_pairs={{0,64},{8,72},{16,80},{24,88},{32,96},{40,104},{48,112},{56,120},{... | collective-permute-start | bytes 184328 | tf_op jit(solution)/shard_map/ppermute | solution.py:35
  112.6 27.8 %collective-permute-start.7 = (bf16[160,1408]{1,0:T(8,128)(2,1)}, bf16[160,1408]{1,0:T(8,128)(2,1)}, u32[]{:S(2)}, u32[]{:S(2)}) collective-permute-start(bf16[160,1408]{1,0:T(8,128)(2,1)} %collective-permute-done.6.refs_0_.refs_1_), channel_id=1, source_target_pairs={{0,32},{8,40},{16,48},{24,56},{32,64},{40,72},{48,80},{56,88},{64,... | collective-permute-start | bytes 1351688 | tf_op jit(solution)/shard_map/ppermute | solution.py:35
  117.3 21.1 %collective-permute-start.21 = (bf16[160,960]{1,0:T(8,128)(2,1)}, bf16[160,960]{1,0:T(8,128)(2,1)}, u32[]{:S(2)}, u32[]{:S(2)}) collective-permute-start(bf16[160,960]{1,0:T(8,128)(2,1)} %constant_dynamic-update-slice_fusion.2.refs_4_), channel_id=1, source_target_pairs={{0,24},{8,0},{16,8},{24,16},{32,56},{40,32},{48,40},{56,48},{64,88... | collective-permute-start | bytes 921608 | tf_op jit(solution)/shard_map/ppermute | solution.py:35
  122.8 15.6 %collective-permute-start.20 = (bf16[160,960]{1,0:T(8,128)(2,1)}, bf16[160,960]{1,0:T(8,128)(2,1)}, u32[]{:S(2)}, u32[]{:S(2)}) collective-permute-start(bf16[160,960]{1,0:T(8,128)(2,1)} %constant_dynamic-update-slice_fusion.2.refs_4_), channel_id=1, source_target_pairs={{0,16},{8,24},{16,0},{24,8},{32,48},{40,56},{48,32},{56,40},{64,80... | collective-permute-start | bytes 921608 | tf_op jit(solution)/shard_map/ppermute | solution.py:35
  126.3 12.1 %collective-permute-start.19 = (bf16[160,960]{1,0:T(8,128)(2,1)}, bf16[160,960]{1,0:T(8,128)(2,1)}, u32[]{:S(2)}, u32[]{:S(2)}) collective-permute-start(bf16[160,960]{1,0:T(8,128)(2,1)} %constant_dynamic-update-slice_fusion.2.refs_4_), channel_id=1, source_target_pairs={{0,8},{8,16},{16,24},{24,0},{32,40},{40,48},{48,56},{56,32},{64,72... | collective-permute-start | bytes 921608 | tf_op jit(solution)/shard_map/ppermute | solution.py:35
  143.8 24.9 %collective-permute-start.22 = (bf16[160,2048]{1,0:T(8,128)(2,1)S(1)}, bf16[160,2048]{1,0:T(8,128)(2,1)S(1)}, u32[]{:S(2)}, u32[]{:S(2)}) collective-permute-start(bf16[160,2048]{1,0:T(8,128)(2,1)S(1)} %down.5), channel_id=1, source_target_pairs={{0,1},{1,0},{2,3},{3,2},{4,5},{5,4},{6,7},{7,6},{8,9},{9,8},{10,11... | collective-permute-start | bytes 1966088 | tf_op jit(solution)/shard_map/ppermute | solution.py:420
  169.7 14.7 %all-to-all-start = ((bf16[4,40,2048]{2,1,0:T(8,128)(2,1)}), bf16[4,40,2048]{2,1,0:T(8,128)(2,1)}, u32[]{:S(2)}, u32[]{:S(2)}) async-start(bf16[4,40,2048]{2,1,0:T(8,128)(2,1)} %copy-done.5), calls=%async_computation | async-start | bytes 1310720 | tf_op jit(solution)/shard_map/all_to_all | solution.py:425
  (53 other events, 1199.1 us)

commit v2 on v1

--- a/solution.py
+++ b/solution.py
@@ -390,19 +390,38 @@
     mixed = jnp.dot(deviation, pool_ref[...], preferred_element_type=F32)
     mixed = mixed * scale_ref[...].astype(F32)
     mixed = by_core(core, [mixed[i * tile : (i + 1) * tile] for i in range(8)]).astype(BF)
+    keep_ref[...] = mixed[: rows // 2]
+    send_ref[...] = mixed[rows // 2 :]
+
+
+def spread_kernel(m_ref, w_ref, out_ref):
+    m = m_ref[...]
     for at in range(0, w_ref.shape[0], 256):
-        share = lax.dot_general(
-            mixed, w_ref[at : at + 256, 128:256], (((1,), (1,)), ((), ())), preferred_element_type=F32
+        out_ref[:, at : at + 256] = lax.dot_general(
+            m, w_ref[at : at + 256, 128:256], (((1,), (1,)), ((), ())), preferred_element_type=F32
         ).astype(BF)
-        keep_ref[:, at : at + 256] = share[: rows // 2]
-        send_ref[:, at : at + 256] = share[rows // 2 :]
+
+
+def spread(mixed, w):
+    rows, depth = mixed.shape[0], w.shape[0]
+    return pl.pallas_call(
+        spread_kernel,
+        out_shape=jax.ShapeDtypeStruct((rows, depth), BF),
+        in_specs=[VMEM] * 2,
+        out_specs=VMEM,
+        compiler_params=limit(6),
+        cost_estimate=pl.CostEstimate(
+            flops=2 * rows * depth * 128, bytes_accessed=2 << 20, transcendentals=0
+        ),
+        name="spread",
+    )(mixed, w)
 
 
 def mixer(kind, mine, other, w, pool_w, pool_scale):
     rows, depth = 2 * other.shape[0], other.shape[1]
     return pl.pallas_call(
         mixer_kernel,
-        out_shape=(jax.ShapeDtypeStruct((rows // 2, depth), BF),) * 2,
+        out_shape=(jax.ShapeDtypeStruct((rows // 2, 128), BF),) * 2,
         in_specs=[SMEM] + [VMEM] * 5,
         out_specs=(VMEM, VMEM),
         compiler_params=limit(14),
@@ -478,8 +497,10 @@
     stream, copies = settle(parts, stream, gains, 1, 0.5)
     kind = jnp.stack([numbers[2], numbers[1]])
     mine, other = rows_of_all(copies)
-    share = mixer(kind, pooled(mine, mix_w), other, mix_w, pool_w[0], pool_scale[None])
-    stream, copies = settle(shares_of_rows(*share), stream, gains, 3, 1.0)
+    mine = pooled(mine, mix_w)
+    mine, other = mixer(kind, mine, other, mix_w, pool_w[0], pool_scale[None])
+    other, mine = spread(other, mix_w), spread(mine, mix_w)
+    stream, copies = settle(shares_of_rows(mine, other), stream, gains, 3, 1.0)
     mine, other = rows_of_all(copies)
     hidden, gate_up = gated(mine, payloads, width)
     other = gated(other, [gate_up], width)

time: 268 us -> 267 us (level)
  transfers between devices with their start and end apart: 28 -> 28, of which waited for: 12 -> 12; matrix products, arithmetic and copies ran while one was open for 5% -> 5% of each run, Pallas kernels for 5% -> 6%
where the time goes in v2:
time: 267 us; the launch traced here: 265 us
  starting transfers between devices  117 us (44%)
  blocking collectives  62.1 us (23%)
  waiting for transfers between devices  30.8 us (12%)
  Pallas kernels  27.2 us (10%)
  local copies, waits for them, and re-layouts  27 us (10%)
    ppermute x22, starting transfers between devices, shift(): return lax.ppermute(array, 'fs', fs_shift(dy, dz))  77 us
    ppermute x5, starting transfers between devices, core_swap(): return lax.ppermute(array, 'tp', [(k, k ^ 1) for k in range(8)])  35.5 us
    all_to_all x2, blocking collectives, shares_of_rows(): lax.all_to_all(tiles, 'tp', 0, 0, tiled=True, axis_index_groups=X_GROUPS)  26.3 us
    all_to_all x2, blocking collectives, rows_of_all(): lax.all_to_all(copies, 'tp', 0, 0, tiled=True, axis_index_groups=X_GROUPS)  24.7 us
    unnamed x112, local copies, waits for them, and re-layouts  23.2 us
    ppermute x22, waiting for transfers between devices, shift(): return lax.ppermute(array, 'fs', fs_shift(dy, dz))  18.3 us
    all_gather x1, blocking collectives, body(): lax.all_gather(first, 'fs', axis=0, tiled=True, axis_index_groups=groups)  11.1 us
    all_to_all x1, waiting for transfers between devices, shares_of_rows(): lax.all_to_all(tiles, 'tp', 0, 0, tiled=True, axis_index_groups=X_GROUPS)  9.41 us
  transfers between devices with their start and end apart: 28, of which 12 were waited for; matrix products, arithmetic and copies ran while one was open for 5% of the time, Pallas kernels for 6%

profile of v2, /device:TPU:1, one launch (start us, length us, event | category | flops | bytes accessed | tf_op | source)
XLA Modules:
  0.0 265.1 jit_solution(6113978254677038147)
XLA Ops:
  1.7 11.1 %all_gather.3 = bf16[128,1408]{1,0:T(8,128)(2,1)S(1)} all-gather(bf16[32,1408]{1,0:T(8,128)(2,1)} %get-tuple-element.21), channel_id=1, replica_groups={{0,8,16,24},{32,40,48,56},{64,72,80,88},{96,104,112,120},{128,136,144,1..., dimensions={0}, use_global_device_ids=true | all-gather | bytes 450560 | tf_op jit(solution)/shard_map/all_gather | solution.py:463
  13.7 12.1 %collective-permute-start.8 = (bf16[160,1408]{1,0:T(8,128)(2,1)S(1)}, bf16[160,1408]{1,0:T(8,128)(2,1)S(1)}, u32[]{:S(2)}, u32[]{:S(2)}) collective-permute-start(bf16[160,1408]{1,0:T(8,128)(2,1)S(1)} %constant_dynamic-update-slice_fusion.refs_0_.refs_8_), channel_id=1, source_target_pairs={{0,480},{8,488},{16,496},{24,504},{32,0},{40,8},{48,16},{56,24},{6... | collective-permute-start | bytes 1351688 | tf_op jit(solution)/shard_map/ppermute | solution.py:35
  29.4 3.6 %collective-permute-done.8.refs_2_.refs_9_ = bf16[160,1408]{1,0:T(8,128)(2,1)S(1)} collective-permute-done((bf16[160,1408]{1,0:T(8,128)(2,1)S(1)}, bf16[160,1408]{1,0:T(8,128)(2,1)S(1)}, u32[]{:S(2)}, u32[]{:S(2)}) %collective-permute-start.8) | collective-permute-done | bytes 450592 | tf_op jit(solution)/shard_map/ppermute | solution.py:35
  33.0 5.3 %collective-permute-start.9 = (bf16[160,1408]{1,0:T(8,128)(2,1)S(1)}, bf16[160,1408]{1,0:T(8,128)(2,1)S(1)}, u32[]{:S(2)}, u32[]{:S(2)}) collective-permute-start(bf16[160,1408]{1,0:T(8,128)(2,1)S(1)} %collective-permute-done.8.refs_2_.refs_9_), channel_id=1, source_target_pairs={{0,480},{8,488},{16,496},{24,504},{32,0},{40,8},{48,16},{56,24},{6... | collective-permute-start | bytes 1351688 | tf_op jit(solution)/shard_map/ppermute | solution.py:35
  41.5 3.0 %collective-permute-done.9.refs_1_.refs_10_ = bf16[160,1408]{1,0:T(8,128)(2,1)S(1)} collective-permute-done((bf16[160,1408]{1,0:T(8,128)(2,1)S(1)}, bf16[160,1408]{1,0:T(8,128)(2,1)S(1)}, u32[]{:S(2)}, u32[]{:S(2)}) %collective-permute-start.9) | collective-permute-done | bytes 450592 | tf_op jit(solution)/shard_map/ppermute | solution.py:35
  44.5 5.3 %collective-permute-start.10 = (bf16[160,1408]{1,0:T(8,128)(2,1)S(1)}, bf16[160,1408]{1,0:T(8,128)(2,1)S(1)}, u32[]{:S(2)}, u32[]{:S(2)}) collective-permute-start(bf16[160,1408]{1,0:T(8,128)(2,1)S(1)} %collective-permute-done.9.refs_1_.refs_10_), channel_id=1, source_target_pairs={{0,480},{8,488},{16,496},{24,504},{32,0},{40,8},{48,16},{56,24},{6... | collective-permute-start | bytes 1351688 | tf_op jit(solution)/shard_map/ppermute | solution.py:35
  55.2 5.4 %collective-permute-start.11 = (bf16[160,1408]{1,0:T(8,128)(2,1)S(1)}, bf16[160,1408]{1,0:T(8,128)(2,1)S(1)}, u32[]{:S(2)}, u32[]{:S(2)}) collective-permute-start(bf16[160,1408]{1,0:T(8,128)(2,1)S(1)} %collective-permute-done.10.refs_1_.refs_11_), channel_id=1, source_target_pairs={{0,480},{8,488},{16,496},{24,504},{32,0},{40,8},{48,16},{56,24},{6... | collective-permute-start | bytes 1351688 | tf_op jit(solution)/shard_map/ppermute | solution.py:35
  65.9 5.0 %collective-permute-start.12 = (bf16[160,1408]{1,0:T(8,128)(2,1)S(1)}, bf16[160,1408]{1,0:T(8,128)(2,1)S(1)}, u32[]{:S(2)}, u32[]{:S(2)}) collective-permute-start(bf16[160,1408]{1,0:T(8,128)(2,1)S(1)} %collective-permute-done.11.refs_1_.refs_12_), channel_id=1, source_target_pairs={{0,480},{8,488},{16,496},{24,504},{32,0},{40,8},{48,16},{56,24},{6... | collective-permute-start | bytes 1351688 | tf_op jit(solution)/shard_map/ppermute | solution.py:35
  76.3 5.0 %collective-permute-start.13 = (bf16[160,1408]{1,0:T(8,128)(2,1)S(1)}, bf16[160,1408]{1,0:T(8,128)(2,1)S(1)}, u32[]{:S(2)}, u32[]{:S(2)}) collective-permute-start(bf16[160,1408]{1,0:T(8,128)(2,1)S(1)} %collective-permute-done.12.refs_1_.refs_13_), channel_id=1, source_target_pairs={{0,480},{8,488},{16,496},{24,504},{32,0},{40,8},{48,16},{56,24},{6... | collective-permute-start | bytes 1351688 | tf_op jit(solution)/shard_map/ppermute | solution.py:35
  86.4 3.3 %collective-permute-start.17 = (bf16[352,960]{1,0:T(8,128)(2,1)}, bf16[352,960]{1,0:T(8,128)(2,1)S(1)}, u32[]{:S(2)}, u32[]{:S(2)}) collective-permute-start(bf16[352,960]{1,0:T(8,128)(2,1)} %slice_dynamic-update-slice_fusion.3.refs_0_), channel_id=1, source_target_pairs={{0,24},{8,0},{16,8},{24,16},{32,56},{40,32},{48,40},{56,48},{64,88... | collective-permute-start | bytes 2027528 | tf_op jit(solution)/shard_map/ppermute | solution.py:35
  94.2 4.6 %collective-permute-start.14 = (bf16[160,1408]{1,0:T(8,128)(2,1)S(1)}, bf16[160,1408]{1,0:T(8,128)(2,1)S(1)}, u32[]{:S(2)}, u32[]{:S(2)}) collective-permute-start(bf16[160,1408]{1,0:T(8,128)(2,1)S(1)} %collective-permute-done.13.refs_1_.refs_14_), channel_id=1, source_target_pairs={{0,480},{8,488},{16,496},{24,504},{32,0},{40,8},{48,16},{56,24},{6... | collective-permute-start | bytes 1351688 | tf_op jit(solution)/shard_map/ppermute | solution.py:35
  103.5 5.7 %collective-permute-done.6.refs_0_.refs_1_ = bf16[160,1408]{1,0:T(8,128)(2,1)} collective-permute-done((bf16[160,1408]{1,0:T(8,128)(2,1)S(1)}, bf16[160,1408]{1,0:T(8,128)(2,1)}, u32[]{:S(2)}, u32[]{:S(2)}) %collective-permute-start.6) | collective-permute-done | bytes 450592 | tf_op jit(solution)/shard_map/ppermute | solution.py:35
  117.3 4.7 %collective-permute-start.21 = (bf16[160,960]{1,0:T(8,128)(2,1)}, bf16[160,960]{1,0:T(8,128)(2,1)}, u32[]{:S(2)}, u32[]{:S(2)}) collective-permute-start(bf16[160,960]{1,0:T(8,128)(2,1)} %constant_dynamic-update-slice_fusion.2.refs_4_), channel_id=1, source_target_pairs={{0,24},{8,0},{16,8},{24,16},{32,56},{40,32},{48,40},{56,48},{64,88... | collective-permute-start | bytes 921608 | tf_op jit(solution)/shard_map/ppermute | solution.py:35
  122.8 2.6 collective-permute-start.20
  143.8 23.2 %collective-permute-start.22 = (bf16[160,2048]{1,0:T(8,128)(2,1)S(1)}, bf16[160,2048]{1,0:T(8,128)(2,1)S(1)}, u32[]{:S(2)}, u32[]{:S(2)}) collective-permute-start(bf16[160,2048]{1,0:T(8,128)(2,1)S(1)} %down.5), channel_id=1, source_target_pairs={{0,1},{1,0},{2,3},{3,2},{4,5},{5,4},{6,7},{7,6},{8,9},{9,8},{10,11... | collective-permute-start | bytes 1966088 | tf_op jit(solution)/shard_map/ppermute | solution.py:439
  169.7 4.2 %all-to-all-start = ((bf16[4,40,2048]{2,1,0:T(8,128)(2,1)}), bf16[4,40,2048]{2,1,0:T(8,128)(2,1)}, u32[]{:S(2)}, u32[]{:S(2)}) async-start(bf16[4,40,2048]{2,1,0:T(8,128)(2,1)} %copy-done.5), calls=%async_computation | async-start | bytes 1310720 | tf_op jit(solution)/shard_map/all_to_all | solution.py:444
  175.0 9.4 %all-to-all-done.parts_ref = bf16[4,40,2048]{2,1,0:T(8,128)(2,1)} async-done(((bf16[4,40,2048]{2,1,0:T(8,128)(2,1)}), bf16[4,40,2048]{2,1,0:T(8,128)(2,1)}, u32[]{:S(2)}, u32[]{:S(2)}) %all-to-all-start) | async-done | bytes 655392 | tf_op jit(solution)/shard_map/all_to_all | solution.py:444
  185.8 12.5 %all_to_all.25 = bf16[4,40,2048]{2,1,0:T(8,128)(2,1)} all-to-all(bf16[4,40,2048]{2,1,0:T(8,128)(2,1)S(1)} %get-tuple-element.28), channel_id=1, replica_groups={{0,2,4,6},{1,3,5,7},{8,10,12,14},{9,11,13,15},{16,18,20,22},{17,19,21,2..., dimensions={0} | all-to-all | bytes 1310720 | tf_op jit(solution)/shard_map/all_to_all | solution.py:448
  198.3 4.4 %collective-permute-start.23 = (bf16[160,2048]{1,0:T(8,128)(2,1)}, bf16[160,2048]{1,0:T(8,128)(2,1)}, u32[]{:S(2)}, u32[]{:S(2)}) collective-permute-start(bf16[160,2048]{1,0:T(8,128)(2,1)} %bitcast.6.x_ref), channel_id=1, source_target_pairs={{0,1},{1,0},{2,3},{3,2},{4,5},{5,4},{6,7},{7,6},{8,9},{9,8},{10,11... | collective-permute-start | bytes 1966088 | tf_op jit(solution)/shard_map/ppermute | solution.py:439
  211.9 13.3 %all_to_all.26.parts_ref = bf16[4,40,2048]{2,1,0:T(8,128)(2,1)S(1)} all-to-all(bf16[4,40,2048]{2,1,0:T(8,128)(2,1)S(1)} %pair_sum.4), channel_id=1, replica_groups={{0,2,4,6},{1,3,5,7},{8,10,12,14},{9,11,13,15},{16,18,20,22},{17,19,21,2..., dimensions={0} | all-to-all | bytes 1310720 | tf_op jit(solution)/shard_map/all_to_all | solution.py:444
  225.5 12.2 %all_to_all.27 = bf16[4,40,2048]{2,1,0:T(8,128)(2,1)S(1)} all-to-all(bf16[4,40,2048]{2,1,0:T(8,128)(2,1)S(1)} %get-tuple-element.33), channel_id=1, replica_groups={{0,2,4,6},{1,3,5,7},{8,10,12,14},{9,11,13,15},{16,18,20,22},{17,19,21,2..., dimensions={0} | all-to-all | bytes 1310720 | tf_op jit(solution)/shard_map/all_to_all | solution.py:448
  237.7 4.0 %collective-permute-start.25 = (bf16[160,2048]{1,0:T(8,128)(2,1)S(1)}, bf16[160,2048]{1,0:T(8,128)(2,1)S(1)}, u32[]{:S(2)}, u32[]{:S(2)}) collective-permute-start(bf16[160,2048]{1,0:T(8,128)(2,1)S(1)} %bitcast.10), channel_id=1, source_target_pairs={{0,1},{1,0},{2,3},{3,2},{4,5},{5,4},{6,7},{7,6},{8,9},{9,8},{10,11... | collective-permute-start | bytes 1966088 | tf_op jit(solution)/shard_map/ppermute | solution.py:439
  241.8 2.7 gated.2
  251.2 13.0 %all_to_all.28.parts_ref = bf16[4,40,2048]{2,1,0:T(8,128)(2,1)S(1)} all-to-all(bf16[4,40,2048]{2,1,0:T(8,128)(2,1)S(1)} %pair_sum.5), channel_id=1, replica_groups={{0,2,4,6},{1,3,5,7},{8,10,12,14},{9,11,13,15},{16,18,20,22},{17,19,21,2..., dimensions={0} | all-to-all | bytes 1310720 | tf_op jit(solution)/shard_map/all_to_all | solution.py:444
  (186 shorter events, 88.5 us)
Async XLA Ops:
  13.7 19.2 %collective-permute-start.8 = (bf16[160,1408]{1,0:T(8,128)(2,1)S(1)}, bf16[160,1408]{1,0:T(8,128)(2,1)S(1)}, u32[]{:S(2)}, u32[]{:S(2)}) collective-permute-start(bf16[160,1408]{1,0:T(8,128)(2,1)S(1)} %constant_dynamic-update-slice_fusion.refs_0_.refs_8_), channel_id=1, source_target_pairs={{0,480},{8,488},{16,496},{24,504},{32,0},{40,8},{48,16},{56,24},{6... | collective-permute-start | bytes 1351688 | tf_op jit(solution)/shard_map/ppermute | solution.py:35
  25.9 12.4 %collective-permute-start = (bf16[160,1408]{1,0:T(8,128)(2,1)S(1)}, bf16[160,1408]{1,0:T(8,128)(2,1)S(1)}, u32[]{:S(2)}, u32[]{:S(2)}) collective-permute-start(bf16[160,1408]{1,0:T(8,128)(2,1)S(1)} %constant_dynamic-update-slice_fusion.refs_0_.refs_8_), channel_id=1, source_target_pairs={{0,32},{8,40},{16,48},{24,56},{32,64},{40,72},{48,80},{56,88},{64,... | collective-permute-start | bytes 1351688 | tf_op jit(solution)/shard_map/ppermute | solution.py:35
  33.0 11.6 %collective-permute-start.9 = (bf16[160,1408]{1,0:T(8,128)(2,1)S(1)}, bf16[160,1408]{1,0:T(8,128)(2,1)S(1)}, u32[]{:S(2)}, u32[]{:S(2)}) collective-permute-start(bf16[160,1408]{1,0:T(8,128)(2,1)S(1)} %collective-permute-done.8.refs_2_.refs_9_), channel_id=1, source_target_pairs={{0,480},{8,488},{16,496},{24,504},{32,0},{40,8},{48,16},{56,24},{6... | collective-permute-start | bytes 1351688 | tf_op jit(solution)/shard_map/ppermute | solution.py:35
  38.3 11.5 %collective-permute-start.1 = (bf16[160,1408]{1,0:T(8,128)(2,1)S(1)}, bf16[160,1408]{1,0:T(8,128)(2,1)S(1)}, u32[]{:S(2)}, u32[]{:S(2)}) collective-permute-start(bf16[160,1408]{1,0:T(8,128)(2,1)S(1)} %collective-permute-done.refs_1_.refs_7_), channel_id=1, source_target_pairs={{0,32},{8,40},{16,48},{24,56},{32,64},{40,72},{48,80},{56,88},{64,... | collective-permute-start | bytes 1351688 | tf_op jit(solution)/shard_map/ppermute | solution.py:35
  44.5 10.6 %collective-permute-start.10 = (bf16[160,1408]{1,0:T(8,128)(2,1)S(1)}, bf16[160,1408]{1,0:T(8,128)(2,1)S(1)}, u32[]{:S(2)}, u32[]{:S(2)}) collective-permute-start(bf16[160,1408]{1,0:T(8,128)(2,1)S(1)} %collective-permute-done.9.refs_1_.refs_10_), channel_id=1, source_target_pairs={{0,480},{8,488},{16,496},{24,504},{32,0},{40,8},{48,16},{56,24},{6... | collective-permute-start | bytes 1351688 | tf_op jit(solution)/shard_map/ppermute | solution.py:35
  49.9 10.7 %collective-permute-start.2 = (bf16[160,1408]{1,0:T(8,128)(2,1)S(1)}, bf16[160,1408]{1,0:T(8,128)(2,1)S(1)}, u32[]{:S(2)}, u32[]{:S(2)}) collective-permute-start(bf16[160,1408]{1,0:T(8,128)(2,1)S(1)} %collective-permute-done.1.refs_0_.refs_6_), channel_id=1, source_target_pairs={{0,32},{8,40},{16,48},{24,56},{32,64},{40,72},{48,80},{56,88},{64,... | collective-permute-start | bytes 1351688 | tf_op jit(solution)/shard_map/ppermute | solution.py:35
  55.2 10.7 %collective-permute-start.11 = (bf16[160,1408]{1,0:T(8,128)(2,1)S(1)}, bf16[160,1408]{1,0:T(8,128)(2,1)S(1)}, u32[]{:S(2)}, u32[]{:S(2)}) collective-permute-start(bf16[160,1408]{1,0:T(8,128)(2,1)S(1)} %collective-permute-done.10.refs_1_.refs_11_), channel_id=1, source_target_pairs={{0,480},{8,488},{16,496},{24,504},{32,0},{40,8},{48,16},{56,24},{6... | collective-permute-start | bytes 1351688 | tf_op jit(solution)/shard_map/ppermute | solution.py:35
  60.6 10.3 %collective-permute-start.3 = (bf16[160,1408]{1,0:T(8,128)(2,1)S(1)}, bf16[160,1408]{1,0:T(8,128)(2,1)S(1)}, u32[]{:S(2)}, u32[]{:S(2)}) collective-permute-start(bf16[160,1408]{1,0:T(8,128)(2,1)S(1)} %collective-permute-done.2.refs_0_.refs_5_), channel_id=1, source_target_pairs={{0,32},{8,40},{16,48},{24,56},{32,64},{40,72},{48,80},{56,88},{64,... | collective-permute-start | bytes 1351688 | tf_op jit(solution)/shard_map/ppermute | solution.py:35
  65.9 10.4 %collective-permute-start.12 = (bf16[160,1408]{1,0:T(8,128)(2,1)S(1)}, bf16[160,1408]{1,0:T(8,128)(2,1)S(1)}, u32[]{:S(2)}, u32[]{:S(2)}) collective-permute-start(bf16[160,1408]{1,0:T(8,128)(2,1)S(1)} %collective-permute-done.11.refs_1_.refs_12_), channel_id=1, source_target_pairs={{0,480},{8,488},{16,496},{24,504},{32,0},{40,8},{48,16},{56,24},{6... | collective-permute-start | bytes 1351688 | tf_op jit(solution)/shard_map/ppermute | solution.py:35
  70.9 10.7 %collective-permute-start.4 = (bf16[160,1408]{1,0:T(8,128)(2,1)S(1)}, bf16[160,1408]{1,0:T(8,128)(2,1)S(1)}, u32[]{:S(2)}, u32[]{:S(2)}) collective-permute-start(bf16[160,1408]{1,0:T(8,128)(2,1)S(1)} %collective-permute-done.3.refs_0_.refs_4_), channel_id=1, source_target_pairs={{0,32},{8,40},{16,48},{24,56},{32,64},{40,72},{48,80},{56,88},{64,... | collective-permute-start | bytes 1351688 | tf_op jit(solution)/shard_map/ppermute | solution.py:35
  76.3 17.9 %collective-permute-start.13 = (bf16[160,1408]{1,0:T(8,128)(2,1)S(1)}, bf16[160,1408]{1,0:T(8,128)(2,1)S(1)}, u32[]{:S(2)}, u32[]{:S(2)}) collective-permute-start(bf16[160,1408]{1,0:T(8,128)(2,1)S(1)} %collective-permute-done.12.refs_1_.refs_13_), channel_id=1, source_target_pairs={{0,480},{8,488},{16,496},{24,504},{32,0},{40,8},{48,16},{56,24},{6... | collective-permute-start | bytes 1351688 | tf_op jit(solution)/shard_map/ppermute | solution.py:35
  81.6 17.2 %collective-permute-start.5 = (bf16[160,1408]{1,0:T(8,128)(2,1)S(1)}, bf16[160,1408]{1,0:T(8,128)(2,1)S(1)}, u32[]{:S(2)}, u32[]{:S(2)}) collective-permute-start(bf16[160,1408]{1,0:T(8,128)(2,1)S(1)} %collective-permute-done.4.refs_0_.refs_3_), channel_id=1, source_target_pairs={{0,32},{8,40},{16,48},{24,56},{32,64},{40,72},{48,80},{56,88},{64,... | collective-permute-start | bytes 1351688 | tf_op jit(solution)/shard_map/ppermute | solution.py:35
  86.4 35.5 %collective-permute-start.17 = (bf16[352,960]{1,0:T(8,128)(2,1)}, bf16[352,960]{1,0:T(8,128)(2,1)S(1)}, u32[]{:S(2)}, u32[]{:S(2)}) collective-permute-start(bf16[352,960]{1,0:T(8,128)(2,1)} %slice_dynamic-update-slice_fusion.3.refs_0_), channel_id=1, source_target_pairs={{0,24},{8,0},{16,8},{24,16},{32,56},{40,32},{48,40},{56,48},{64,88... | collective-permute-start | bytes 2027528 | tf_op jit(solution)/shard_map/ppermute | solution.py:35
  89.7 35.8 %collective-permute-start.16 = (bf16[352,960]{1,0:T(8,128)(2,1)}, bf16[352,960]{1,0:T(8,128)(2,1)S(1)}, u32[]{:S(2)}, u32[]{:S(2)}) collective-permute-start(bf16[352,960]{1,0:T(8,128)(2,1)} %slice_dynamic-update-slice_fusion.3.refs_0_), channel_id=1, source_target_pairs={{0,16},{8,24},{16,0},{24,8},{32,48},{40,56},{48,32},{56,40},{64,80... | collective-permute-start | bytes 2027528 | tf_op jit(solution)/shard_map/ppermute | solution.py:35
  92.2 46.2 %collective-permute-start.15 = (bf16[352,960]{1,0:T(8,128)(2,1)}, bf16[352,960]{1,0:T(8,128)(2,1)}, u32[]{:S(2)}, u32[]{:S(2)}) collective-permute-start(bf16[352,960]{1,0:T(8,128)(2,1)} %slice_dynamic-update-slice_fusion.3.refs_0_), channel_id=1, source_target_pairs={{0,8},{8,16},{16,24},{24,0},{32,40},{40,48},{48,56},{56,32},{64,72... | collective-permute-start | bytes 2027528 | tf_op jit(solution)/shard_map/ppermute | solution.py:35
  94.2 18.4 %collective-permute-start.14 = (bf16[160,1408]{1,0:T(8,128)(2,1)S(1)}, bf16[160,1408]{1,0:T(8,128)(2,1)S(1)}, u32[]{:S(2)}, u32[]{:S(2)}) collective-permute-start(bf16[160,1408]{1,0:T(8,128)(2,1)S(1)} %collective-permute-done.13.refs_1_.refs_14_), channel_id=1, source_target_pairs={{0,480},{8,488},{16,496},{24,504},{32,0},{40,8},{48,16},{56,24},{6... | collective-permute-start | bytes 1351688 | tf_op jit(solution)/shard_map/ppermute | solution.py:35
  98.8 10.5 %collective-permute-start.6 = (bf16[160,1408]{1,0:T(8,128)(2,1)S(1)}, bf16[160,1408]{1,0:T(8,128)(2,1)}, u32[]{:S(2)}, u32[]{:S(2)}) collective-permute-start(bf16[160,1408]{1,0:T(8,128)(2,1)S(1)} %collective-permute-done.5.refs_0_.refs_2_), channel_id=1, source_target_pairs={{0,32},{8,40},{16,48},{24,56},{32,64},{40,72},{48,80},{56,88},{64,... | collective-permute-start | bytes 1351688 | tf_op jit(solution)/shard_map/ppermute | solution.py:35
  109.2 7.4 %collective-permute-start.18 = (bf16[32,960]{1,0:T(8,128)(2,1)S(1)}, bf16[32,960]{1,0:T(8,128)(2,1)S(1)}, u32[]{:S(2)}, u32[]{:S(2)}) collective-permute-start(bf16[32,960]{1,0:T(8,128)(2,1)S(1)} %get-tuple-element.37), channel_id=1, source_target_pairs={{0,64},{8,72},{16,80},{24,88},{32,96},{40,104},{48,112},{56,120},{... | collective-permute-start | bytes 184328 | tf_op jit(solution)/shard_map/ppermute | solution.py:35
  112.6 27.8 %collective-permute-start.7 = (bf16[160,1408]{1,0:T(8,128)(2,1)}, bf16[160,1408]{1,0:T(8,128)(2,1)}, u32[]{:S(2)}, u32[]{:S(2)}) collective-permute-start(bf16[160,1408]{1,0:T(8,128)(2,1)} %collective-permute-done.6.refs_0_.refs_1_), channel_id=1, source_target_pairs={{0,32},{8,40},{16,48},{24,56},{32,64},{40,72},{48,80},{56,88},{64,... | collective-permute-start | bytes 1351688 | tf_op jit(solution)/shard_map/ppermute | solution.py:35
  117.3 21.1 %collective-permute-start.21 = (bf16[160,960]{1,0:T(8,128)(2,1)}, bf16[160,960]{1,0:T(8,128)(2,1)}, u32[]{:S(2)}, u32[]{:S(2)}) collective-permute-start(bf16[160,960]{1,0:T(8,128)(2,1)} %constant_dynamic-update-slice_fusion.2.refs_4_), channel_id=1, source_target_pairs={{0,24},{8,0},{16,8},{24,16},{32,56},{40,32},{48,40},{56,48},{64,88... | collective-permute-start | bytes 921608 | tf_op jit(solution)/shard_map/ppermute | solution.py:35
  122.8 15.6 %collective-permute-start.20 = (bf16[160,960]{1,0:T(8,128)(2,1)}, bf16[160,960]{1,0:T(8,128)(2,1)}, u32[]{:S(2)}, u32[]{:S(2)}) collective-permute-start(bf16[160,960]{1,0:T(8,128)(2,1)} %constant_dynamic-update-slice_fusion.2.refs_4_), channel_id=1, source_target_pairs={{0,16},{8,24},{16,0},{24,8},{32,48},{40,56},{48,32},{56,40},{64,80... | collective-permute-start | bytes 921608 | tf_op jit(solution)/shard_map/ppermute | solution.py:35
  126.3 12.1 %collective-permute-start.19 = (bf16[160,960]{1,0:T(8,128)(2,1)}, bf16[160,960]{1,0:T(8,128)(2,1)}, u32[]{:S(2)}, u32[]{:S(2)}) collective-permute-start(bf16[160,960]{1,0:T(8,128)(2,1)} %constant_dynamic-update-slice_fusion.2.refs_4_), channel_id=1, source_target_pairs={{0,8},{8,16},{16,24},{24,0},{32,40},{40,48},{48,56},{56,32},{64,72... | collective-permute-start | bytes 921608 | tf_op jit(solution)/shard_map/ppermute | solution.py:35
  143.8 24.9 %collective-permute-start.22 = (bf16[160,2048]{1,0:T(8,128)(2,1)S(1)}, bf16[160,2048]{1,0:T(8,128)(2,1)S(1)}, u32[]{:S(2)}, u32[]{:S(2)}) collective-permute-start(bf16[160,2048]{1,0:T(8,128)(2,1)S(1)} %down.5), channel_id=1, source_target_pairs={{0,1},{1,0},{2,3},{3,2},{4,5},{5,4},{6,7},{7,6},{8,9},{9,8},{10,11... | collective-permute-start | bytes 1966088 | tf_op jit(solution)/shard_map/ppermute | solution.py:439
  169.7 14.7 %all-to-all-start = ((bf16[4,40,2048]{2,1,0:T(8,128)(2,1)}), bf16[4,40,2048]{2,1,0:T(8,128)(2,1)}, u32[]{:S(2)}, u32[]{:S(2)}) async-start(bf16[4,40,2048]{2,1,0:T(8,128)(2,1)} %copy-done.5), calls=%async_computation | async-start | bytes 1310720 | tf_op jit(solution)/shard_map/all_to_all | solution.py:444
  (53 other events, 1203.6 us)
